TPU v7x, 512 devices: a whole 4x4x16 slice. The times are simulated.
512 devices in a mesh: sp: 32 (over z, core), tp: 16 (over y, x).
Axes of the slice: x: 4, y: 4, z: 16, core: 2. Of those that a mesh axis runs over, the one named last changes fastest.
Arguments:
- cotangent: bfloat16 [4096, 2048], P('sp'), may hold values from -6 to 6
- normed: bfloat16 [4096, 2048], P('sp'), may hold values from -6 to 6
- inverse_root_mean_square: float32 [4096], P('sp'), may hold values from 0.5 to 2
- expert_norm_scale: float32 [2048], replicated, may hold values from 0.1 to 1.9
- routes: int32 [4096, 2], P('sp'), may hold values from 0 to 31, all different within a row; in each aligned block of 128 rows (0 to 127, 128 to 255, ...) at most 16 rows name the same one
- route_probability_weight: float32 [4096, 2], P('sp'), may hold values from 0.2 to 1
- gate_weight: bfloat16 [32, 2048, 2048], P('sp', None, 'tp'), may hold values from -0.125 to 0.125
- up_weight: bfloat16 [32, 2048, 2048], P('sp', None, 'tp'), may hold values from -0.125 to 0.125
- down_weight: bfloat16 [32, 2048, 2048], P('sp', 'tp'), may hold values from -0.125 to 0.125
- recurrence_input: bfloat16 [4096, 1024], P('sp', 'tp'), may hold values from -6 to 6
- recurrence_gate_logits: bfloat16 [4096, 1024], P('sp', 'tp'), may hold values from -6 to 6
- input_gate_logits: bfloat16 [4096, 1024], P('sp', 'tp'), may hold values from -6 to 6
- channel_decay_weight: float32 [1024], P('tp'), may hold values from 3 to 20
- extra_log_decay: float32 [4096, 1024], P('sp', 'tp'), may hold values from -1 to 0
- output_matrix: bfloat16 [2048, 1024], P(None, 'tp'), may hold values from -0.1875 to 0.1875
Outputs:
- grad_gate: bfloat16 [32, 2048, 2048], P('sp', None, 'tp')
- grad_up: bfloat16 [32, 2048, 2048], P('sp', None, 'tp')
- grad_down: bfloat16 [32, 2048, 2048], P('sp', 'tp')
- grad_out_weight: float32 [2048, 1024], P('sp', 'tp')
- grad_rec_input: float32 [4096, 1024], P('sp', 'tp')
- grad_decay_gate: float32 [4096, 1024], P('sp', 'tp')
- grad_input_gate: float32 [4096, 1024], P('sp', 'tp')
Inputs may be any that keep to these rules, and one draw needn't show every extreme that they name: `routes`: each row names 2 different experts; among the rows of one device no expert is named more than 16 times.
All inputs are finite; a program needn't handle non-finite values.
Results may differ from a plain program's by a relative error of at most 0.025.
Values may be sent and summed in bfloat16 or wider, within the bound.
A program may use at most 64 MiB of HBM per device.

v0:
```python
import jax
import jax.numpy as jnp
from jax import lax
from jax.sharding import Mesh
from jax.sharding import PartitionSpec as P

TP = ("tp_0", "tp_1")


def side_by_side(arrays, axis, split_dim, concat_dim, along):
    both = jnp.concatenate(arrays, axis=along)
    filled, at, gathered = (
        lax.all_to_all(both, axis, split_axis=split_dim, concat_axis=concat_dim, tiled=True),
        0,
        [],
    )
    for a in arrays:
        gathered.append(lax.slice_in_dim(filled, at, at + a.shape[along], axis=along))
        at += a.shape[along]
    return tuple(gathered)


def in_blocks(value, dim, count):
    dims = value.shape
    parts = value.reshape(*dims[:dim], count, dims[dim] // count, *dims[dim + 1 :])
    return jnp.moveaxis(parts, dim, 0)


def sum_at_owner(value, axis, dim):
    parts = in_blocks(value, dim, lax.axis_size(axis))
    arrived = lax.all_to_all(parts, axis, split_axis=0, concat_axis=0, tiled=True)
    return arrived.astype(jnp.float32).sum(axis=0)


def over_axes(value, axes):
    for axis in axes:
        value = lax.psum(value, axis)
    return value


def in_order(parts, dim):
    parts = jnp.moveaxis(parts, 0, dim)
    dims = parts.shape
    return parts.reshape(*dims[:dim], dims[dim] * dims[dim + 1], *dims[dim + 2 :])


def sent_to_all(value, axis):
    count = lax.axis_size(axis)
    return lax.all_to_all(
        jnp.broadcast_to(value[None], (count, *value.shape)), axis, 0, 0, tiled=True
    )


def gathered_copies(value, axis, dim):
    return in_order(sent_to_all(value, axis), dim)


def gathered_once(value, axis):
    leaves = jax.tree.leaves(value)
    sequence = sorted(range(len(leaves)), key=lambda k: -leaves[k].size)
    width = (1, *leaves[sequence[0]].shape)[-1]
    lines = [
        jnp.pad(leaves[k].reshape(-1), (0, -leaves[k].size % width)).reshape(-1, width)
        for k in sequence
    ]
    both, at, found = (sent_to_all(jnp.concatenate(lines), axis), 0, {})
    for k, line in zip(sequence, lines):
        section = both[:, at : at + len(line)].reshape(len(both), -1)
        found[k] = section[:, : leaves[k].size].reshape(-1, *leaves[k].shape)
        at += len(line)
    numbers = iter(range(len(leaves)))
    return jax.tree.map(lambda _: found[next(numbers)], value)


def joined_by_halves(pieces, combine):
    while len(jax.tree.leaves(pieces)[0]) > 1:
        pieces = jax.vmap(combine)(
            *(jax.tree.map(lambda part: part[side::2], pieces) for side in (0, 1))
        )
    return jax.tree.map(lambda part: part[0], pieces)


def entering(value, axis, combine, identity, reverse):
    count, here = (lax.axis_size(axis), lax.axis_index(axis))
    passed = jnp.arange(count) > here if reverse else jnp.arange(count) < here

    def kept(part, zero, own):
        part = jnp.where(
            passed.reshape(-1, *(1 for _ in own.shape)), part, jnp.asarray(zero, own.dtype)
        )
        return part[::-1] if reverse else part

    pieces = gathered_once(value, axis)
    return joined_by_halves(jax.tree.map(kept, pieces, identity, value), combine)


def link(earlier, later):
    return (earlier[0] * later[0], later[0] * earlier[1] + later[1])


def shards(
    cotangent,
    normed,
    inverse_root_mean_square,
    expert_norm_scale,
    routes,
    route_probability_weight,
    gate_weight,
    up_weight,
    down_weight,
    recurrence_input,
    recurrence_gate_logits,
    input_gate_logits,
    channel_decay_weight,
    extra_log_decay,
    output_matrix,
):
    tok_rows, features = normed.shape
    groups = lax.axis_size("sp")
    picks = routes.shape[1]
    capacity = 2 * picks * tok_rows // groups
    rowdims = (((0,), (0,)), ((), ()))
    coldims = (((1,), (1,)), ((), ()))
    chosen = routes.reshape(-1)
    member = (chosen[:, None] == jnp.arange(groups, dtype=jnp.int32)[None, :]).astype(jnp.int32)
    ranking = jnp.sum((jnp.cumsum(member, axis=0) - member) * member, axis=1)
    landing = chosen * capacity + ranking
    scaled = (
        route_probability_weight[:, :, None] * cotangent[:, None, :].astype(jnp.float32)
    ).astype(jnp.bfloat16)
    scaled = scaled.reshape(tok_rows * picks, features)
    copies = jnp.repeat(normed, picks, axis=0)
    grad_send = jnp.zeros((groups * capacity, features), jnp.bfloat16).at[landing].set(scaled)
    token_send = jnp.zeros((groups * capacity, features), jnp.bfloat16).at[landing].set(copies)
    grad_recv, token_recv = side_by_side((grad_send, token_send), "sp", 0, 0, 1)
    gate_w = gate_weight[0]
    up_w = up_weight[0]
    down_w = down_weight[0]
    gate_pre = jnp.dot(token_recv, gate_w, preferred_element_type=jnp.float32)
    up_pre = jnp.dot(token_recv, up_w, preferred_element_type=jnp.float32)
    sigma = jax.nn.sigmoid(gate_pre)
    swish = gate_pre * sigma
    active = (swish * up_pre).astype(jnp.bfloat16)
    d_active = lax.dot_general(grad_recv, down_w, coldims, preferred_element_type=jnp.float32)
    d_gate = (d_active * up_pre * sigma * (1.0 + gate_pre * (1.0 - sigma))).astype(jnp.bfloat16)
    d_up = (d_active * swish).astype(jnp.bfloat16)
    grad_down = lax.dot_general(
        active, grad_recv, rowdims, preferred_element_type=jnp.float32
    ).astype(jnp.bfloat16)
    grad_gate = lax.dot_general(
        token_recv, d_gate, rowdims, preferred_element_type=jnp.float32
    ).astype(jnp.bfloat16)
    grad_up = lax.dot_general(token_recv, d_up, rowdims, preferred_element_type=jnp.float32).astype(
        jnp.bfloat16
    )
    partial_rows = lax.dot_general(d_gate, gate_w, coldims, preferred_element_type=jnp.float32)
    partial_rows = partial_rows + lax.dot_general(
        d_up, up_w, coldims, preferred_element_type=jnp.float32
    )
    shared = sum_at_owner(partial_rows.astype(jnp.bfloat16), TP, 1).astype(jnp.bfloat16)
    returned = lax.all_to_all(shared, "sp", split_axis=0, concat_axis=0, tiled=True)
    slice_width = returned.shape[1]
    offset = lax.axis_index(TP) * slice_width
    gain_part = lax.dynamic_slice_in_dim(expert_norm_scale, offset, slice_width, 0)
    normed_part = lax.dynamic_slice_in_dim(normed, offset, slice_width, 1)
    cot_part = lax.dynamic_slice_in_dim(cotangent, offset, slice_width, 1)
    d_norm = jnp.sum(
        returned[landing].astype(jnp.float32).reshape(tok_rows, picks, slice_width), axis=1
    )
    nhat = normed_part.astype(jnp.float32) / gain_part[None, :]
    gained = gain_part[None, :] * d_norm
    stat = over_axes(jnp.sum(gained * nhat, axis=1), TP)[:, None] / features
    mix_part = (
        cot_part.astype(jnp.float32) + inverse_root_mean_square[:, None] * (gained - nhat * stat)
    ).astype(jnp.bfloat16)
    d_mix = gathered_copies(mix_part, TP, 1)
    retention_factor = jax.nn.sigmoid(recurrence_gate_logits.astype(jnp.float32))
    admit = jax.nn.sigmoid(input_gate_logits.astype(jnp.float32))
    signal = recurrence_input.astype(jnp.float32)
    decay_speed = jax.nn.softplus(-channel_decay_weight)
    log_retention = -8.0 * retention_factor * decay_speed[None, :] + extra_log_decay
    keep = jnp.exp(log_retention)
    scale_in = jnp.sqrt(-jnp.expm1(2.0 * log_retention))
    driven = scale_in * admit * signal
    channels = keep.shape[1]
    identity = (jnp.ones((channels,), jnp.float32), jnp.zeros((channels,), jnp.float32))
    keep_cum, state_loc = lax.associative_scan(link, (keep, driven), axis=0)
    _, state_in = entering((keep_cum[-1], state_loc[-1]), "sp", link, identity, False)
    state = state_loc + keep_cum * state_in[None, :]
    hidden = state.astype(jnp.bfloat16)
    state_prev = jnp.concatenate([state_in[None, :], state[:-1]], axis=0)
    grad_out_weight = sum_at_owner(
        lax.dot_general(d_mix, hidden, rowdims, preferred_element_type=jnp.float32).astype(
            jnp.bfloat16
        ),
        "sp",
        0,
    )
    d_state = jnp.dot(d_mix, output_matrix, preferred_element_type=jnp.float32)
    keep_next = jnp.concatenate([keep[1:], jnp.ones((1, channels), jnp.float32)], axis=0)
    tail_keep, grad_loc = lax.associative_scan(link, (keep_next, d_state), reverse=True, axis=0)
    block_map = (keep[0] * tail_keep[0], keep[0] * grad_loc[0])
    _, grad_enter = entering(block_map, "sp", link, identity, True)
    total = grad_loc + tail_keep * grad_enter[None, :]
    grad_rec_input = total * scale_in * admit
    grad_input_gate = total * scale_in * signal * admit * (1.0 - admit)
    d_log = total * state_prev * keep - total * admit * signal * keep * keep / scale_in
    grad_decay_gate = (
        d_log * (-8.0 * decay_speed[None, :]) * retention_factor * (1.0 - retention_factor)
    )
    return (
        grad_gate[None],
        grad_up[None],
        grad_down[None],
        grad_out_weight,
        grad_rec_input,
        grad_decay_gate,
        grad_input_gate,
    )


def solution(mesh):
    finer = Mesh(mesh.devices.reshape(mesh.shape["sp"], 4, 4), ("sp", "tp_0", "tp_1"))
    placed = (
        P("sp", None),
        P("sp", None),
        P("sp"),
        P(),
        P("sp", None),
        P("sp", None),
        P("sp", None, TP),
        P("sp", None, TP),
        P("sp", TP, None),
        P("sp", TP),
        P("sp", TP),
        P("sp", TP),
        P(TP),
        P("sp", TP),
        P(None, TP),
    )
    return jax.shard_map(
        shards,
        mesh=finer,
        in_specs=placed,
        out_specs=(
            P("sp", None, TP),
            P("sp", None, TP),
            P("sp", TP, None),
            P("sp", TP),
            P("sp", TP),
            P("sp", TP),
            P("sp", TP),
        ),
        check_vma=False,
    )
```

profile of v0, /device:TPU:1, one launch (start us, length us, event | category | flops | bytes accessed | tf_op | source)
XLA Modules:
  0.0 428.7 jit_solution(14606756271678646964)
XLA Ops:
  3.6 1.7 broadcast_in_dim.73
  5.3 1.2 reshape.155
  6.5 2.4 mul.410
  8.9 2.7 mul.411
  12.0 4.4 %scatter_custom_fusion.1 = bf16[512,2048]{1,0:T(8,128)(2,1)} fusion(s32[256]{0:T(256)S(1)} %bitcast.130, bf16[256,2048]{1,0:T(8,128)(2,1)} %reshape.155, bf16[]{:T(256)} %constant.16.clone.1), kind=kCustom, calls=%fused_computation.27 | custom fusion | bytes 2097664 | tf_op jit(solution)/shard_map/scatter | solution.py:134
  16.4 3.8 scatter_custom_fusion
  20.2 2.7 pad_maximum_fusion
  22.9 207.6 %all_to_all.49 = bf16[32,16,4096]{2,1,0:T(8,128)(2,1)S(1)} all-to-all(bf16[32,16,4096]{2,1,0:T(8,128)(2,1)S(1)} %bitcast.99), channel_id=1, replica_groups=mesh['sp'=32,'tp_0'=4,'tp_1'=4] {'sp'}, dimensions={0} | all-to-all | bytes 8388608 | tf_op jit(solution)/shard_map/all_to_all | solution.py:13
  235.9 34.0 %all_to_all.50 = bf16[16,512,128]{2,1,0:T(8,128)(2,1)S(1)} all-to-all(bf16[16,512,128]{2,1,0:T(8,128)(2,1)S(1)} %bitcast.100), channel_id=1, replica_groups=mesh['sp'=32,'tp_0'=4,'tp_1'=4] {'tp_0','tp_1'}, dimensions={0} | all-to-all | bytes 4194304 | tf_op jit(solution)/shard_map/all_to_all | solution.py:31
  270.9 5.5 %all-to-all-start.2 = ((bf16[32,16,128]{2,1,0:T(8,128)(2,1)}), bf16[32,16,128]{2,1,0:T(8,128)(2,1)S(1)}, u32[]{:S(2)}, u32[]{:S(2)}) async-start(bf16[32,16,128]{2,1,0:T(8,128)(2,1)} %bitcast.12), calls=%async_computation.2 | async-start | bytes 262144 | tf_op jit(solution)/shard_map/all_to_all | solution.py:161
  277.2 15.4 %all-to-all-done.2 = bf16[32,16,128]{2,1,0:T(8,128)(2,1)S(1)} async-done(((bf16[32,16,128]{2,1,0:T(8,128)(2,1)}), bf16[32,16,128]{2,1,0:T(8,128)(2,1)S(1)}, u32[]{:S(2)}, u32[]{:S(2)}) %all-to-all-start.2) | async-done | bytes 131104 | tf_op jit(solution)/shard_map/all_to_all | solution.py:161
  294.6 6.6 %psum.14 = f32[128]{0:T(128)S(1)} all-reduce(f32[128]{0:T(128)S(1)} %multiply_reduce_fusion), channel_id=1, replica_groups=mesh['sp'=32,'tp_0'=4,'tp_1'=4] {'tp_0'}, use_global_device_ids=true, to_apply=%region_8.9 | all-reduce | flops 128 | bytes 1024 | tf_op jit(solution)/shard_map/psum | solution.py:37
  301.1 6.7 %psum.15 = f32[128]{0:T(128)S(1)} all-reduce(f32[128]{0:T(128)S(1)} %psum.14), channel_id=1, replica_groups=mesh['sp'=32,'tp_0'=4,'tp_1'=4] {'tp_1'}, use_global_device_ids=true, to_apply=%region_9.10 | all-reduce | flops 128 | bytes 1024 | tf_op jit(solution)/shard_map/psum | solution.py:37
  309.8 3.7 all-to-all-start.3
  317.6 4.8 %all-to-all-done.3 = bf16[16,128,128]{1,2,0:T(8,128)(2,1)S(1)} async-done(((bf16[16,128,128]{1,2,0:T(8,128)(2,1)}), bf16[16,128,128]{1,2,0:T(8,128)(2,1)S(1)}, u32[]{:S(2)}, u32[]{:S(2)}) %all-to-all-start.3) | async-done | bytes 524320 | tf_op jit(solution)/shard_map/all_to_all | solution.py:49
  338.3 10.2 %all-to-all-start.6 = ((f32[32,1,128]{2,1,0:T(1,128)}), f32[32,1,128]{2,1,0:T(1,128)S(1)}, u32[]{:S(2)}, u32[]{:S(2)}) async-start(f32[32,1,128]{2,1,0:T(1,128)} %reshape.170), calls=%async_computation.6 | async-start | bytes 32768 | tf_op jit(solution)/shard_map/all_to_all | solution.py:49
  348.6 11.5 %all-to-all-done.6 = f32[32,1,128]{2,1,0:T(1,128)S(1)} async-done(((f32[32,1,128]{2,1,0:T(1,128)}), f32[32,1,128]{2,1,0:T(1,128)S(1)}, u32[]{:S(2)}, u32[]{:S(2)}) %all-to-all-start.6) | async-done | bytes 16416 | tf_op jit(solution)/shard_map/all_to_all | solution.py:49
  379.9 15.4 %all_to_all.51 = f32[32,1,128]{2,1,0:T(1,128)S(1)} all-to-all(f32[32,1,128]{2,1,0:T(1,128)S(1)} %reshape.166), channel_id=1, replica_groups=mesh['sp'=32,'tp_0'=4,'tp_1'=4] {'sp'}, dimensions={0} | all-to-all | bytes 32768 | tf_op jit(solution)/shard_map/all_to_all | solution.py:49
  399.9 1.1 reshape.168
  401.0 4.8 %all-to-all-start.5 = ((bf16[32,2,2048]{2,1,0:T(2,128)(2,1)}), bf16[32,2,2048]{2,1,0:T(2,128)(2,1)S(1)}, u32[]{:S(2)}, u32[]{:S(2)}) async-start(bf16[32,2,2048]{2,1,0:T(2,128)(2,1)} %reshape.168), calls=%async_computation.5 | async-start | bytes 524288 | tf_op jit(solution)/shard_map/all_to_all | solution.py:31
  405.8 3.3 fusion
  409.1 3.2 fusion.1
  412.3 1.3 fusion.2
  414.3 13.0 %all-to-all-done.5 = bf16[32,2,2048]{2,1,0:T(2,128)(2,1)S(1)} async-done(((bf16[32,2,2048]{2,1,0:T(2,128)(2,1)}), bf16[32,2,2048]{2,1,0:T(2,128)(2,1)S(1)}, u32[]{:S(2)}, u32[]{:S(2)}) %all-to-all-start.5) | async-done | bytes 262176 | tf_op jit(solution)/shard_map/all_to_all | solution.py:31
  (353 shorter events, 58.9 us)
Async XLA Ops:
  0.6 229.8 %copy-start = (bf16[1,2048,128]{2,1,0:T(8,128)(2,1)S(1)}, bf16[1,2048,128]{2,1,0:T(8,128)(2,1)}, u32[]{:S(2)}) copy-start(bf16[1,2048,128]{2,1,0:T(8,128)(2,1)} %param.21) | copy-start | bytes 1572868
  0.6 5.9 %copy-start.3 = (bf16[128,2048]{1,0:T(8,128)(2,1)S(1)}, bf16[128,2048]{1,0:T(8,128)(2,1)}, u32[]{:S(2)}) copy-start(bf16[128,2048]{1,0:T(8,128)(2,1)} %param.15) | copy-start | bytes 1572868
  8.9 2.7 copy-start.10
  230.5 2.1 copy-start.1
  230.5 1.4 copy-start.4
  231.9 2.0 copy-start.14
  231.9 1.3 copy-start.12
  233.2 0.7 copy-start.16
  269.9 37.9 %copy-start.11 = (f32[128]{0:T(128)S(1)}, f32[128]{0:T(128)}, u32[]{:S(2)}) copy-start(f32[128]{0:T(128)} %param.17) | copy-start | bytes 1540
  269.9 43.6 %copy-start.13 = (f32[64]{0:T(128)S(1)}, f32[64]{0:T(128)}, u32[]{:S(2)}) copy-start(f32[64]{0:T(128)} %param.27) | copy-start | bytes 772
  269.9 43.6 %copy-start.5 = (f32[128,64]{0,1:T(8,128)S(1)}, f32[128,64]{0,1:T(8,128)}, u32[]{:S(2)}) copy-start(f32[128,64]{0,1:T(8,128)} %param.28) | copy-start | bytes 98308
  269.9 43.6 %copy-start.7 = (bf16[128,64]{0,1:T(8,128)(2,1)S(1)}, bf16[128,64]{0,1:T(8,128)(2,1)}, u32[]{:S(2)}) copy-start(bf16[128,64]{0,1:T(8,128)(2,1)} %param.25) | copy-start | bytes 49156
  270.9 51.6 %copy-start.6 = (bf16[2048,64]{0,1:T(8,128)(2,1)S(1)}, bf16[2048,64]{0,1:T(8,128)(2,1)}, u32[]{:S(2)}) copy-start(bf16[2048,64]{0,1:T(8,128)(2,1)} %param.29) | copy-start | bytes 786436
  270.9 21.8 %all-to-all-start.2 = ((bf16[32,16,128]{2,1,0:T(8,128)(2,1)}), bf16[32,16,128]{2,1,0:T(8,128)(2,1)S(1)}, u32[]{:S(2)}, u32[]{:S(2)}) async-start(bf16[32,16,128]{2,1,0:T(8,128)(2,1)} %bitcast.12), calls=%async_computation.2 | async-start | bytes 262144 | tf_op jit(solution)/shard_map/all_to_all | solution.py:161
  309.8 12.7 %all-to-all-start.3 = ((bf16[16,128,128]{1,2,0:T(8,128)(2,1)}), bf16[16,128,128]{1,2,0:T(8,128)(2,1)S(1)}, u32[]{:S(2)}, u32[]{:S(2)}) async-start(bf16[16,128,128]{1,2,0:T(8,128)(2,1)} %broadcast_in_dim.77), calls=%async_computation.3 | async-start | bytes 1048576 | tf_op jit(solution)/shard_map/all_to_all | solution.py:49
  334.6 29.8 %copy-start.8 = (bf16[128,64]{0,1:T(8,128)(2,1)S(1)}, bf16[128,64]{0,1:T(8,128)(2,1)}, u32[]{:S(2)}) copy-start(bf16[128,64]{0,1:T(8,128)(2,1)} %param.24) | copy-start | bytes 49156
  334.6 29.8 %copy-start.9 = (bf16[128,64]{0,1:T(8,128)(2,1)S(1)}, bf16[128,64]{0,1:T(8,128)(2,1)}, u32[]{:S(2)}) copy-start(bf16[128,64]{0,1:T(8,128)(2,1)} %param.26) | copy-start | bytes 49156
  338.3 21.9 %all-to-all-start.6 = ((f32[32,1,128]{2,1,0:T(1,128)}), f32[32,1,128]{2,1,0:T(1,128)S(1)}, u32[]{:S(2)}, u32[]{:S(2)}) async-start(f32[32,1,128]{2,1,0:T(1,128)} %reshape.170), calls=%async_computation.6 | async-start | bytes 32768 | tf_op jit(solution)/shard_map/all_to_all | solution.py:49
  401.0 26.3 %all-to-all-start.5 = ((bf16[32,2,2048]{2,1,0:T(2,128)(2,1)}), bf16[32,2,2048]{2,1,0:T(2,128)(2,1)S(1)}, u32[]{:S(2)}, u32[]{:S(2)}) async-start(bf16[32,2,2048]{2,1,0:T(2,128)(2,1)} %reshape.168), calls=%async_computation.5 | async-start | bytes 524288 | tf_op jit(solution)/shard_map/all_to_all | solution.py:31
  405.7 6.5 %copy-start.2 = (bf16[32,16,4096]{2,1,0:T(8,128)(2,1)S(1)}, bf16[32,16,4096]{2,1,0:T(8,128)(2,1)}, u32[]{:S(2)}) copy-start(bf16[32,16,4096]{2,1,0:T(8,128)(2,1)} %copy-done.1) | copy-start | bytes 12582916
  409.1 3.2 copy-start.15
  409.1 3.2 copy-start.17
where the time goes:
time: 436 us; the launch traced here: 429 us
  blocking collectives  270 us (62%)
  local copies, waits for them, and re-layouts  57.2 us (13%)
  waiting for transfers between devices  44.8 us (10%)
  starting transfers between devices  24.2 us (6%)
  other arithmetic  17.6 us (4%)
  matrix products  11.9 us (3%)
    all_to_all x1, blocking collectives, side_by_side(): lax.all_to_all(both, axis, split_axis=split_dim, concat_axis=concat_dim,...  208 us
    all_to_all x1, blocking collectives, sum_at_owner(): lax.all_to_all(parts, axis, split_axis=0, concat_axis=0, tiled=True)  34 us
    all_to_all x2, waiting for transfers between devices, sent_to_all(): lax.all_to_all(jnp.broadcast_to(value[None], (count, *value.shape)), axis...  16.4 us
    all_to_all x1, waiting for transfers between devices, shards(): lax.all_to_all(shared, 'sp', split_axis=0, concat_axis=0, tiled=True)  15.4 us
    all_to_all x1, blocking collectives, sent_to_all(): lax.all_to_all(jnp.broadcast_to(value[None], (count, *value.shape)), axis...  15.4 us
    all_to_all x2, starting transfers between devices, sent_to_all(): lax.all_to_all(jnp.broadcast_to(value[None], (count, *value.shape)), axis...  13.9 us
    psum x2, blocking collectives, over_axes(): value = lax.psum(value, axis)  13.3 us
    all_to_all x1, waiting for transfers between devices, sum_at_owner(): lax.all_to_all(parts, axis, split_axis=0, concat_axis=0, tiled=True)  13 us
  transfers between devices with their start and end apart: 4, of which 4 were waited for; matrix products, arithmetic and copies ran while one was open for 3% of the time, Pallas kernels for 0%

commit v1 on v0

v1 whole, which is shorter than its diff:
```python
import functools

import jax
import jax.numpy as jnp
from jax import lax
from jax.experimental import pallas as pl
from jax.experimental.pallas import tpu as pltpu
from jax.sharding import PartitionSpec as P

MESH = pl.DeviceIdType.MESH
F32 = jnp.float32
BF16 = jnp.bfloat16
SIDE = 4
SHIFT = 3
COLS = 128
CAP = 16


def dot(a, b, ca, cb):
    return lax.dot_general(a, b, (((ca,), (cb,)), ((), ())), preferred_element_type=F32)


def take(ref, sem):
    pltpu.make_async_copy(ref, ref, sem).wait()


def send(src, dst, send_sem, recv_sem, target):
    pltpu.make_async_remote_copy(
        src_ref=src,
        dst_ref=dst,
        send_sem=send_sem,
        recv_sem=recv_sem,
        device_id=target,
        device_id_type=MESH,
    ).start()


class Gather:
    def __init__(self, block, i, axis_to, ss, rs):
        self.block, self.i, self.to, self.ss, self.rs = block, i, axis_to, ss, rs
        self.up, self.down, self.far = lax.rem(i + 1, 4), lax.rem(i + 3, 4), lax.rem(i + 2, 4)

    def go(self, src, half, target, k):
        ref = self.block(src, half)
        send(ref, ref, self.ss.at[k], self.rs.at[k], target)

    def first(self):
        self.go(self.i, None, self.to(self.up), 0)
        self.go(self.i, None, self.to(self.down), 1)

    def relay(self):
        take(self.block(self.down, None), self.rs.at[0])
        self.go(self.down, 0, self.to(self.up), 2)
        take(self.block(self.up, None), self.rs.at[1])
        self.go(self.up, 1, self.to(self.down), 3)

    def last(self):
        take(self.block(self.far, 0), self.rs.at[2])
        take(self.block(self.far, 1), self.rs.at[3])

    def sent(self):
        take(self.block(self.i, None), self.ss.at[0])
        take(self.block(self.i, None), self.ss.at[1])
        take(self.block(self.down, 0), self.ss.at[2])
        take(self.block(self.up, 1), self.ss.at[3])


class Scatter:
    def __init__(self, block, i, axis_to, ss, rs, part, low, high):
        self.block, self.i, self.to, self.ss, self.rs = block, i, axis_to, ss, rs
        self.part, self.low, self.high = part, low, high
        self.up, self.down, self.far = lax.rem(i + 1, 4), lax.rem(i + 3, 4), lax.rem(i + 2, 4)

    def go(self, src, dst, target, k):
        send(src, dst, self.ss.at[k], self.rs.at[k], target)

    def first(self):
        up, down = self.to(self.up), self.to(self.down)
        self.go(self.block(self.far, 0), self.part(0), up, 0)
        self.go(self.block(self.far, 1), self.part(1), down, 1)
        self.go(self.block(self.up, 1), self.low(1), up, 2)
        self.go(self.block(self.down, 0), self.high(0), down, 3)

    def relay(self):
        for k, (member, target, half, dst) in enumerate(
            ((self.up, self.up, 0, self.low(0)), (self.down, self.down, 1, self.high(1)))
        ):
            take(self.part(half), self.rs.at[k])
            ref = self.block(member, half)
            ref[...] = (ref[...].astype(F32) + self.part(half)[...].astype(F32)).astype(BF16)
            self.go(ref, dst, self.to(target), 4 + k)

    def last(self):
        take(self.low(1), self.rs.at[2])
        take(self.high(0), self.rs.at[3])
        take(self.low(0), self.rs.at[4])
        take(self.high(1), self.rs.at[5])

    def total(self, half):
        return (
            self.block(self.i, half)[...].astype(F32)
            + self.low(half)[...].astype(F32)
            + self.high(half)[...].astype(F32)
        )

    def sent(self):
        for k in range(6):
            take(self.part(0), self.ss.at[k])


def softplus(v):
    z = jnp.exp(-jnp.abs(v))
    s = z / (2.0 + z)
    q = s * s
    series = jnp.zeros_like(s)
    for k in range(9, -1, -1):
        series = series * q + 1.0 / (2 * k + 1)
    return jnp.maximum(v, 0.0) + 2.0 * s * series


def expm1(v):
    near = jnp.clip(v, -0.5, 0.5)
    series = jnp.ones_like(v)
    for k in range(10, 1, -1):
        series = 1.0 + near * series * (1.0 / k)
    return jnp.where(jnp.abs(v) < 0.5, near * series, jnp.exp(v) - 1.0)


def kernel(
    ns,
    cot,
    norm,
    irms,
    gain,
    routes,
    prob,
    gate_w,
    up_w,
    down_w,
    rec_in,
    rec_gate,
    in_gate,
    decay_w,
    extra,
    out_m,
    g_gate,
    g_up,
    g_down,
    g_out,
    g_rec,
    g_dec,
    g_in,
    packed,
    picked,
    rows,
    wide,
    d_wide,
    act,
    part,
    t_buf,
    lo_buf,
    hi_buf,
    s_buf,
    t2_buf,
    lo2_buf,
    hi2_buf,
    back,
    arrived,
    dn,
    d_mix,
    scan_a,
    scan_b,
    rows_f,
    lead,
    leads,
    trail,
    trails,
    coef,
    gw_all,
    gw_pair,
    gw_chip,
    gw_in,
    z_s,
    z_r,
    ag_s,
    ag_r,
    rs_s,
    rs_r,
    dn_s,
    dn_r,
    back_s,
    back_r,
    lead_s,
    lead_r,
    trail_s,
    trail_r,
    pair_s,
    pair_r,
    gw_s,
    gw_r,
):
    sp, tp = lax.axis_index("sp"), lax.axis_index("tp")
    z, core = lax.div(sp, 2), lax.rem(sp, 2)
    y, x = lax.div(tp, SIDE), lax.rem(tp, SIDE)
    nz = ns // 2
    tokens = norm.shape[0]
    near = nz // 2
    chunk = near * 2 * CAP

    def to_x(v):
        return {"sp": sp, "tp": y * SIDE + v}

    def to_y(v):
        return {"sp": sp, "tp": v * SIDE + x}

    def to_sp(v):
        return {"sp": v, "tp": tp}

    barrier = pltpu.get_barrier_semaphore()
    steps = [1, -1, 2, -2, 3, -3]
    steps = [d for d in steps] + [-4] + [4, 5, -5, 6, -6, 7, -7, 8]
    others = [(0, 1)] + [(d, c) for d in steps for c in (0, 1)]

    def other(d, c):
        if d == 0:
            return z * 2 + (1 - core)
        return lax.rem(z + d + nz, nz) * 2 + c

    for d, c in others:
        pl.semaphore_signal(barrier, inc=1, device_id=to_sp(other(d, c)), device_id_type=MESH)
    for v in (1, 3):
        pl.semaphore_signal(
            barrier, inc=1, device_id=to_x(lax.rem(x + v, SIDE)), device_id_type=MESH
        )
        pl.semaphore_signal(
            barrier, inc=1, device_id=to_y(lax.rem(y + v, SIDE)), device_id_type=MESH
        )

    mine = pl.ds(pl.multiple_of(tp * COLS, COLS), COLS)
    lane = lax.broadcasted_iota(jnp.int32, (tokens, ns), 1)
    chosen = [routes[:, k : k + 1] for k in (0, 1)]
    member = [(e == lane).astype(F32) for e in chosen]
    earlier = (
        lax.broadcasted_iota(jnp.int32, (tokens, tokens), 1)
        < lax.broadcasted_iota(jnp.int32, (tokens, tokens), 0)
    ).astype(BF16)
    before = dot(earlier, (member[0] + member[1]).astype(BF16), 1, 0)
    slot = lax.broadcasted_iota(jnp.int32, (tokens, ns * CAP), 1).astype(F32)
    at = [
        slot
        == (e.astype(F32) * CAP + jnp.sum(m * before, axis=1, keepdims=True))
        for e, m in zip(chosen, member)
    ]
    one = [a.astype(F32) for a in at]
    both = (one[0] + one[1]).astype(BF16)
    picked[...] = both
    own_cot = cot[:, mine].astype(F32)
    packed[0] = dot(both, norm[:, mine], 0, 0).astype(BF16)
    packed[1] = (
        dot(one[0].astype(BF16), (prob[:, 0:1] * own_cot).astype(BF16), 0, 0)
        + dot(one[1].astype(BF16), (prob[:, 1:2] * own_cot).astype(BF16), 0, 0)
    ).astype(BF16)

    pl.semaphore_wait(barrier, len(others) + 4)

    own_x = pl.ds(pl.multiple_of(x * COLS, COLS), COLS)

    def place(d):
        return lax.rem(SHIFT - d + 2 * nz, nz) if not isinstance(d, int) else (SHIFT - d) % nz

    def rows_at(pos, c):
        return pl.ds(pl.multiple_of((pos * 2 + c) * CAP, CAP), CAP)

    for d, c in others:
        target = other(d, c)
        k = 0 if place(d) < near else 1
        send(
            packed.at[:, pl.ds(pl.multiple_of(target * CAP, CAP), CAP), :],
            rows.at[:, y, rows_at(place(d), core), own_x],
            z_s.at[k],
            z_r.at[k],
            to_sp(target),
        )
    pltpu.make_async_copy(
        packed.at[:, pl.ds(pl.multiple_of(sp * CAP, CAP), CAP), :],
        rows.at[:, y, rows_at(SHIFT, core), own_x],
        z_r.at[0],
    ).start()

    channels = extra.shape[1]
    retain = jax.nn.sigmoid(rec_gate[...].astype(F32))
    admit = jax.nn.sigmoid(in_gate[...].astype(F32))
    signal = rec_in[...].astype(F32)
    speed = -8.0 * softplus(-decay_w[...])
    log_keep = retain * speed + extra[...]
    keep = jnp.exp(log_keep)
    scale_in = jnp.sqrt(-expm1(2.0 * log_keep))
    pad = 64
    scan_a[pl.ds(0, pad), :] = jnp.ones((pad, channels), F32)
    scan_a[pl.ds(pad + tokens, pad), :] = jnp.ones((pad, channels), F32)
    scan_b[pl.ds(0, pad), :] = jnp.zeros((pad, channels), F32)
    scan_b[pl.ds(pad + tokens, pad), :] = jnp.zeros((pad, channels), F32)
    body = pl.ds(pad, tokens)

    def scan(a, b, sign):
        step = 1
        while step < tokens:
            scan_a[body, :] = a
            scan_b[body, :] = b
            moved = pl.ds(pad - sign * step, tokens)
            b = a * scan_b[moved, :] + b
            a = a * scan_a[moved, :]
            step *= 2
        return a, b

    keep_cum, state_loc = scan(keep, scale_in * admit * signal, 1)
    lead[...] = jnp.concatenate(
        [keep_cum[tokens - 1 :, :], state_loc[tokens - 1 :, :]], axis=1
    )
    leads[sp] = lead[...]
    for d, c in others:
        send(lead, leads.at[sp], lead_s, lead_r, to_sp(other(d, c)))
    scan_a[body, :] = keep
    keep_next = scan_a[pl.ds(pad + 1, tokens), :]
    rows_f[0] = keep_cum
    rows_f[1] = state_loc
    rows_f[2] = keep
    rows_f[3] = keep_next
    rows_f[4] = scale_in * admit
    rows_f[5] = scale_in * signal * admit * (1.0 - admit)
    rows_f[6] = admit * signal * keep * keep / scale_in
    rows_f[7] = speed * retain * (1.0 - retain)
    wide[:, :COLS] = gate_w[0]
    wide[:, COLS:] = up_w[0]

    def z_arrived(k):
        take(rows.at[:, y, pl.ds(k * chunk, chunk), own_x], z_r.at[k])

    def gathers(k):
        base, half_rows = k * chunk, chunk // 2

        def span(half):
            if half is None:
                return pl.ds(base, chunk)
            return pl.ds(base + half * half_rows, half_rows)

        def at_x(i):
            return pl.ds(pl.multiple_of(i * COLS, COLS), COLS)

        blocks = (
            (lambda i, h: rows.at[0, y, span(h), at_x(i)], x, to_x),
            (lambda i, h: rows.at[1, i, span(h), own_x], y, to_y),
            (lambda i, h: rows.at[0, i, span(h), :], y, to_y),
            (lambda i, h: rows.at[1, :, span(h), at_x(i)], x, to_x),
        )
        made = [
            Gather(b, i, to, ag_s.at[4 * k + n], ag_r.at[4 * k + n])
            for n, (b, i, to) in enumerate(blocks)
        ]
        return made[:2], made[2:]

    def expert(k):
        span = pl.ds(k * chunk, chunk)
        deep = rows.shape[3]
        hidden = jnp.zeros((chunk, 2 * COLS), F32)
        d_act = jnp.zeros((chunk, COLS), F32)
        for j in range(SIDE):
            hidden += dot(rows[0, j, span, :], wide[j * deep : (j + 1) * deep, :], 1, 0)
            d_act += dot(rows[1, j, span, :], down_w[0, :, j * deep : (j + 1) * deep], 1, 1)
        gate_pre, up_pre = hidden[:, :COLS], hidden[:, COLS:]
        sigma = jax.nn.sigmoid(gate_pre)
        swish = gate_pre * sigma
        act[span, :] = (swish * up_pre).astype(BF16)
        d_wide[span, :COLS] = (
            d_act * up_pre * sigma * (1.0 + gate_pre * (1.0 - sigma))
        ).astype(BF16)
        d_wide[span, COLS:] = (d_act * swish).astype(BF16)
        for j in range(SIDE):
            for i in range(0, SIDE, 2):
                low = (j * SIDE + i) * COLS
                piece = dot(d_wide[span, :], wide[low : low + 2 * COLS, :], 1, 1).astype(BF16)
                part[j, i, span, :] = piece[:, :COLS]
                part[j, i + 1, span, :] = piece[:, COLS:]

    def scatters(k):
        base, half, quarter = k * chunk, chunk // 2, chunk // 4

        def span(start, h):
            return pl.ds(start + h * quarter, quarter)

        def full(buf, n):
            return lambda h: buf.at[n, :, pl.ds(h * quarter, quarter), :]

        def flat(buf, n):
            return lambda h: buf.at[n, pl.ds(h * quarter, quarter), :]

        n = 2 * k
        made = (
            Scatter(
                lambda i, h: part.at[:, i, span(base, h), :], x, to_x,
                rs_s.at[4 * k], rs_r.at[4 * k],
                lambda h: t_buf.at[n, h], full(lo_buf, n), full(hi_buf, n),
            ),
            Scatter(
                lambda i, h: part.at[i, :, span(base + half, h), :], y, to_y,
                rs_s.at[4 * k + 1], rs_r.at[4 * k + 1],
                lambda h: t_buf.at[n + 1, h], full(lo_buf, n + 1), full(hi_buf, n + 1),
            ),
            Scatter(
                lambda i, h: s_buf.at[n, i, pl.ds(h * quarter, quarter), :], y, to_y,
                rs_s.at[4 * k + 2], rs_r.at[4 * k + 2],
                lambda h: t2_buf.at[n, h], flat(lo2_buf, n), flat(hi2_buf, n),
            ),
            Scatter(
                lambda i, h: s_buf.at[n + 1, i, pl.ds(h * quarter, quarter), :], x, to_x,
                rs_s.at[4 * k + 3], rs_r.at[4 * k + 3],
                lambda h: t2_buf.at[n + 1, h], flat(lo2_buf, n + 1), flat(hi2_buf, n + 1),
            ),
        )
        return made[:2], made[2:]

    def between(k, first):
        quarter = chunk // 4
        for n, ring in enumerate(first):
            for h in (0, 1):
                s_buf[2 * k + n, :, pl.ds(h * quarter, quarter), :] = ring.total(h).astype(BF16)

    def give_back(k, second):
        half, quarter = chunk // 2, chunk // 4
        for n, ring in enumerate(second):
            for h in (0, 1):
                back[pl.ds(k * chunk + n * half + h * quarter, quarter), :] = ring.total(h).astype(
                    BF16
                )
        dst = arrived.at[pl.ds(pl.multiple_of(sp * CAP, CAP), CAP), :]
        for d, c in others:
            pos = place(-d)
            if (pos < near) != (k == 0):
                continue
            where = rows_at(pos, 1 - core if d == 0 else c)
            send(back.at[where, :], dst, back_s.at[k], back_r, to_sp(other(d, c)))
        if k == 0:
            pltpu.make_async_copy(back.at[rows_at(SHIFT, core), :], dst, back_r).start()

    def each(rings, name):
        for ring in rings:
            getattr(ring, name)()

    a0, b0 = gathers(0)
    a1, b1 = gathers(1)
    r0, q0 = scatters(0)
    r1, q1 = scatters(1)

    z_arrived(0)
    each(a0, "first")
    each(a0, "relay")
    each(a0, "last")
    each(b0, "first")
    z_arrived(1)
    each(a1, "first")
    each(b0, "relay")
    each(a1, "relay")
    each(b0, "last")
    each(a1, "last")
    each(b1, "first")
    expert(0)
    each(r0, "first")
    each(b1, "relay")
    each(r0, "relay")
    each(r0, "last")
    between(0, r0)
    each(q0, "first")
    each(b1, "last")
    expert(1)
    each(r1, "first")
    each(q0, "relay")
    each(q0, "last")
    give_back(0, q0)
    each(r1, "relay")
    each(r1, "last")
    between(1, r1)
    each(q1, "first")
    each(q1, "relay")
    each(q1, "last")
    give_back(1, q1)

    deep = rows.shape[3]
    for j in range(SIDE):
        grads = dot(rows[0, j], d_wide[...], 0, 0).astype(BF16)
        g_gate[0, j * deep : (j + 1) * deep, :] = grads[:, :COLS]
        g_up[0, j * deep : (j + 1) * deep, :] = grads[:, COLS:]
        g_down[0, :, j * deep : (j + 1) * deep] = dot(act[...], rows[1, j], 0, 0).astype(BF16)

    take(leads.at[pl.ds(0, ns - 1)], lead_r)
    state_in = jnp.zeros((1, channels), F32)
    for i in range(ns):
        v = leads[i]
        state_in = jnp.where(i < sp, v[:, :channels] * state_in + v[:, channels:], state_in)
    run = jnp.ones((1, channels), F32)
    for i in range(ns):
        coef[i] = jnp.where(i > sp, run, 0.0)
        run = jnp.where(i > sp, run * leads[i][:, :channels], run)
    state = rows_f[1] + rows_f[0] * state_in
    scan_b[body, :] = state
    first_row = lax.broadcasted_iota(jnp.int32, (tokens, channels), 0) == 0
    state_prev = jnp.where(first_row, state_in, scan_b[pl.ds(pad - 1, tokens), :])
    rows_f[6] = (state_prev * rows_f[2] - rows_f[6]) * rows_f[7]
    hidden = state.astype(BF16)

    take(arrived, back_r)
    dn[y, :, own_x] = dot(picked[...], arrived[...], 1, 0).astype(BF16)
    half = tokens // 2
    quarter = tokens // 4

    def at_x(i):
        return pl.ds(pl.multiple_of(i * COLS, COLS), COLS)

    def piece(start, h):
        return pl.ds(start, half) if h is None else pl.ds(start + h * quarter, quarter)

    shapes = (
        (lambda i, h: dn.at[y, piece(0, h), at_x(i)], x, to_x),
        (lambda i, h: dn.at[i, piece(half, h), own_x], y, to_y),
        (lambda i, h: dn.at[i, piece(0, h), :], y, to_y),
        (lambda i, h: dn.at[:, piece(half, h), at_x(i)], x, to_x),
    )
    dg = [Gather(b, i, to, dn_s.at[n], dn_r.at[n]) for n, (b, i, to) in enumerate(shapes)]
    for pair in (dg[:2], dg[2:]):
        each(pair, "first")
        each(pair, "relay")
        each(pair, "last")

    eye = lax.broadcasted_iota(jnp.int32, (tokens, tokens), 0) == lax.broadcasted_iota(
        jnp.int32, (tokens, tokens), 1
    )
    inv_rms = jnp.sum(jnp.where(eye, irms[...], 0.0), axis=1, keepdims=True)
    stat = jnp.zeros((tokens, 1), F32)
    for j in range(SIDE):
        cols = pl.ds(j * deep, deep)
        g = gain[:, cols]
        stat += jnp.sum(
            (g * dn[j].astype(F32)) * (norm[:, cols].astype(F32) / g), axis=1, keepdims=True
        )
    stat = stat / norm.shape[1]
    for j in range(SIDE):
        cols = pl.ds(j * deep, deep)
        g = gain[:, cols]
        mix = cot[:, cols].astype(F32) + inv_rms * (
            g * dn[j].astype(F32) - (norm[:, cols].astype(F32) / g) * stat
        )
        d_mix[:, cols] = mix.astype(BF16)

    d_state = dot(d_mix[...], out_m[...], 1, 0)
    tail, grad_loc = scan(rows_f[3], d_state, -1)
    first_grad = rows_f[2][:1, :] * grad_loc[:1, :]
    trail[...] = jnp.concatenate([first_grad, first_grad], axis=1)
    trails[sp] = trail[...]
    for d, c in others:
        send(trail, trails.at[sp], trail_s, trail_r, to_sp(other(d, c)))

    g_rows = g_out.shape[0]
    gw = dot(d_mix[...], hidden, 0, 0).astype(BF16)
    for n in range(ns):
        low = n * g_rows
        gw_all[n % 2, n // 2] = jnp.concatenate(
            [gw[low : low + g_rows // 2, :], gw[low + g_rows // 2 : low + g_rows, :]], axis=1
        )
    send(gw_all.at[1 - core], gw_pair, pair_s, pair_r, to_sp(z * 2 + 1 - core))
    take(trails.at[pl.ds(0, ns - 1)], trail_r)
    entering = jnp.zeros((1, channels), F32)
    for i in range(ns):
        entering += coef[i] * trails[i][:, :channels]
    total = grad_loc + tail * entering
    take(gw_pair, pair_r)
    gw_chip[...] = (gw_all[core].astype(F32) + gw_pair[...].astype(F32)).astype(BF16)
    for d in steps:
        zz = lax.rem(z + d + nz, nz)
        send(gw_chip.at[zz], gw_in.at[z], gw_s, gw_r, to_sp(zz * 2 + core))
    pltpu.make_async_copy(gw_chip.at[z], gw_in.at[z], gw_r).start()
    g_rec[...] = total * rows_f[4]
    g_in[...] = total * rows_f[5]
    g_dec[...] = total * rows_f[6]
    take(gw_in, gw_r)
    acc = jnp.zeros((g_rows // 2, 2 * channels), F32)
    for i in range(nz):
        acc += gw_in[i].astype(F32)
    g_out[: g_rows // 2, :] = acc[:, :channels]
    g_out[g_rows // 2 :, :] = acc[:, channels:]

    block = ns // 2 * CAP
    take(packed.at[:, pl.ds(0, block - CAP), :], z_s.at[0])
    take(packed.at[:, pl.ds(0, block), :], z_s.at[1])
    for ring in a0 + b0 + a1 + b1 + list(r0) + list(q0) + list(r1) + list(q1) + dg:
        ring.sent()
    take(back.at[pl.ds(0, block - CAP), :], back_s.at[0])
    take(back.at[pl.ds(0, block), :], back_s.at[1])
    take(leads.at[pl.ds(0, ns - 1)], lead_s)
    take(trails.at[pl.ds(0, ns - 1)], trail_s)
    take(gw_pair, pair_s)
    take(gw_in.at[pl.ds(0, nz - 1)], gw_s)


def shards(
    cotangent,
    normed,
    inverse_root_mean_square,
    expert_norm_scale,
    routes,
    route_probability_weight,
    gate_weight,
    up_weight,
    down_weight,
    recurrence_input,
    recurrence_gate_logits,
    input_gate_logits,
    channel_decay_weight,
    extra_log_decay,
    output_matrix,
):
    ns = lax.axis_size("sp")
    tokens, features = normed.shape
    channels = recurrence_input.shape[1]
    slots = ns * CAP
    chunk, quarter = slots // 2, slots // 8
    wide = features // SIDE
    vmem, dma = pltpu.VMEM, pltpu.SemaphoreType.DMA
    args = (
        cotangent,
        normed,
        inverse_root_mean_square.reshape(1, tokens),
        expert_norm_scale.reshape(1, features),
        routes,
        route_probability_weight,
        gate_weight,
        up_weight,
        down_weight,
        recurrence_input,
        recurrence_gate_logits,
        input_gate_logits,
        channel_decay_weight.reshape(1, channels),
        extra_log_decay,
        output_matrix,
    )
    f32_rows = jax.ShapeDtypeStruct((tokens, channels), F32)
    return pl.pallas_call(
        functools.partial(kernel, ns),
        out_shape=(
            jax.ShapeDtypeStruct(gate_weight.shape, BF16),
            jax.ShapeDtypeStruct(up_weight.shape, BF16),
            jax.ShapeDtypeStruct(down_weight.shape, BF16),
            jax.ShapeDtypeStruct((features // ns, channels), F32),
            f32_rows,
            f32_rows,
            f32_rows,
        ),
        in_specs=[pl.BlockSpec(memory_space=pltpu.VMEM)] * len(args),
        out_specs=[pl.BlockSpec(memory_space=pltpu.VMEM)] * 7,
        scratch_shapes=[
            vmem((2, slots, COLS), BF16),
            vmem((tokens, slots), BF16),
            vmem((2, SIDE, slots, wide), BF16),
            vmem((features, 2 * COLS), BF16),
            vmem((slots, 2 * COLS), BF16),
            vmem((slots, COLS), BF16),
            vmem((SIDE, SIDE, slots, COLS), BF16),
            vmem((4, 2, SIDE, quarter, COLS), BF16),
            vmem((4, SIDE, 2 * quarter, COLS), BF16),
            vmem((4, SIDE, 2 * quarter, COLS), BF16),
            vmem((4, SIDE, 2 * quarter, COLS), BF16),
            vmem((4, 2, quarter, COLS), BF16),
            vmem((4, 2 * quarter, COLS), BF16),
            vmem((4, 2 * quarter, COLS), BF16),
            vmem((slots, COLS), BF16),
            vmem((slots, COLS), BF16),
            vmem((SIDE, tokens, wide), BF16),
            vmem((tokens, features), BF16),
            vmem((tokens + 128, channels), F32),
            vmem((tokens + 128, channels), F32),
            vmem((8, tokens, channels), F32),
            vmem((1, 2 * channels), F32),
            vmem((ns, 1, 2 * channels), F32),
            vmem((1, 2 * channels), F32),
            vmem((ns, 1, 2 * channels), F32),
            vmem((ns, 1, channels), F32),
            vmem((2, ns // 2, features // ns // 2, 2 * channels), BF16),
            vmem((ns // 2, features // ns // 2, 2 * channels), BF16),
            vmem((ns // 2, features // ns // 2, 2 * channels), BF16),
            vmem((ns // 2, features // ns // 2, 2 * channels), BF16),
            dma((2,)),
            dma((2,)),
            dma((8, 4)),
            dma((8, 4)),
            dma((8, 6)),
            dma((8, 6)),
            dma((4, 4)),
            dma((4, 4)),
            dma((2,)),
            dma,
            dma,
            dma,
            dma,
            dma,
            dma,
            dma,
            dma,
            dma,
        ],
        compiler_params=pltpu.CompilerParams(
            collective_id=0, has_side_effects=True, vmem_limit_bytes=60 * 1024 * 1024
        ),
    )(*args)


def solution(mesh):
    placed = (
        P("sp", None),
        P("sp", None),
        P("sp"),
        P(),
        P("sp", None),
        P("sp", None),
        P("sp", None, "tp"),
        P("sp", None, "tp"),
        P("sp", "tp", None),
        P("sp", "tp"),
        P("sp", "tp"),
        P("sp", "tp"),
        P("tp"),
        P("sp", "tp"),
        P(None, "tp"),
    )
    return jax.shard_map(
        shards,
        mesh=mesh,
        in_specs=placed,
        out_specs=(
            P("sp", None, "tp"),
            P("sp", None, "tp"),
            P("sp", "tp", None),
            P("sp", "tp"),
            P("sp", "tp"),
            P("sp", "tp"),
            P("sp", "tp"),
        ),
        check_vma=False,
    )
```

time: 436 us -> 143 us (0.33); the launches traced: 429 us -> 143 us
  blocking collectives: 270 us -> 0 us
  Pallas kernels: 0 us -> 125 us
  waiting for transfers between devices: 44.8 us -> 0 us
  local copies, waits for them, and re-layouts: 57.2 us -> 17.3 us
  starting transfers between devices: 24.2 us -> 0 us
  other arithmetic: 17.6 us -> 0 us
  matrix products: 11.9 us -> 0 us
    all_to_all x3 -> x0, blocking collectives: 257 us -> none  [the longest x1 208 us: side_by_side(): lax.all_to_all(both, axis, split_axis=split_dim, concat_axis=concat_dim,...]
    pallas_call x0 -> x1, Pallas kernels: none -> 125 us  [shards(): pl.pallas_call(functools.partial(kernel, ns), out_shape=(jax.ShapeDtypeSt...]
    all_to_all x4 -> x0, waiting for transfers between devices: 44.8 us -> none  [the longest x2 16.4 us: sent_to_all(): lax.all_to_all(jnp.broadcast_to(value[None], (count, *value.shape)), axis...]
    all_to_all x4 -> x0, starting transfers between devices: 24.2 us -> none  [the longest x2 13.9 us: sent_to_all(): lax.all_to_all(jnp.broadcast_to(value[None], (count, *value.shape)), axis...]
    slice x117 -> x0, local copies, waits for them, and re-layouts: 22.3 us -> none  [the longest x41 8.98 us: shards(): lax.associative_scan(link, (keep_next, d_state), reverse=True, axis=0)]
    psum x2 -> x0, blocking collectives: 13.3 us -> none  [over_axes(): value = lax.psum(value, axis)]
    dot_general x10 -> x0, matrix products: 11.9 us -> none  [the longest x1 3.3 us: shards(): lax.dot_general(token_recv, d_gate, rowdims, preferred_element_type=jnp.f...]
    pad x48 -> x0, local copies, waits for them, and re-layouts: 11.4 us -> none  [the longest x24 5.68 us: shards(): lax.associative_scan(link, (keep_next, d_state), reverse=True, axis=0)]
  transfers between devices with their start and end apart: 4 -> 0, of which waited for: 4 -> 0; matrix products, arithmetic and copies ran while one was open for 3% -> 0% of each run, Pallas kernels for 0% -> 0%
where the time goes in v1:
time: 143 us
  Pallas kernels  125 us (87%)
  local copies, waits for them, and re-layouts  17.3 us (12%)
    pallas_call x1, Pallas kernels, shards(): pl.pallas_call(functools.partial(kernel, ns), out_shape=(jax.ShapeDtypeSt...  125 us
    unnamed x23, local copies, waits for them, and re-layouts  14.4 us
    pallas_call x3, local copies, waits for them, and re-layouts, shards(): pl.pallas_call(functools.partial(kernel, ns), out_shape=(jax.ShapeDtypeSt...  2.96 us

profile of v1, /device:TPU:1, one launch (start us, length us, event | category | flops | bytes accessed | tf_op | source)
XLA Modules:
  0.0 142.6 jit_solution(8058430884140854230)
XLA Ops:
  0.6 0.0 copy-start.2
  0.6 1.5 %copy.24.rec_in = bf16[128,64]{1,0:T(8,128)(2,1)} copy(bf16[128,64]{0,1:T(8,128)(2,1)} %param.24) | data formatting | bytes 32768 | tf_op args[9]
  2.1 1.4 %copy.25.rec_gate = bf16[128,64]{1,0:T(8,128)(2,1)} copy(bf16[128,64]{0,1:T(8,128)(2,1)} %param.25) | data formatting | bytes 32768 | tf_op args[10]
  3.6 1.4 %copy.26.in_gate = bf16[128,64]{1,0:T(8,128)(2,1)} copy(bf16[128,64]{0,1:T(8,128)(2,1)} %param.26) | data formatting | bytes 32768 | tf_op args[11]
  5.0 1.4 copy.22.routes
  6.4 1.4 copy.23.prob
  7.8 1.5 %copy.27.extra = f32[128,64]{1,0:T(8,128)} copy(f32[128,64]{0,1:T(8,128)} %param.28) | data formatting | bytes 65536 | tf_op args[13]
  9.3 0.0 copy-done.2
  9.3 1.0 copy.28.out_m
  10.3 124.6 %shard_map.198 = (bf16[1,2048,128]{2,1,0:T(8,128)(2,1)}, bf16[1,2048,128]{2,1,0:T(8,128)(2,1)}, bf16[1,128,2048]{2,1,0:T(8,128)(2,1)}, f32[64,64]{1,0:T(8,128)},...) custom-call(bf16[128,2048]{1,0:T(8,128)(2,1)} %cot.1, bf16[128,2048]{1,0:T(8,128)(2,1)} %norm.1, ...), custom_call_target="tpu_custom_call" | custom-call | tf_op jit(solution)/shard_map/pallas_call | solution.py:645
  134.9 0.0 copy-start.4
  134.9 1.6 %copy.29 = f32[128,64]{0,1:T(8,128)} copy(f32[128,64]{1,0:T(8,128)} %get-tuple-element.11) | data formatting | bytes 65536 | tf_op jit(solution)/shard_map/pallas_call | solution.py:645
  136.5 0.0 copy-done.4
  136.5 0.0 copy-start.3
  136.5 0.7 copy.30
  137.2 0.1 copy-done.3
  137.3 0.7 copy.31
  138.0 1.9 %copy.36 = bf16[1,2048,128]{2,1,0:T(8,128)(2,1)} copy(bf16[1,2048,128]{2,1,0:T(8,128)(2,1)} %get-tuple-element.21) | data formatting | bytes 1048576
  140.0 0.0 copy-done.1
  140.0 0.8 copy.37
  140.8 0.4 copy-done
  141.2 0.8 copy.38
  142.0 0.0 copy-done.5
  142.0 0.6 copy.39
  (3 shorter events, 0.0 us)
Async XLA Ops:
  0.6 8.7 %copy-start.2 = (bf16[2048,64]{0,1:T(8,128)(2,1)S(1)}, bf16[2048,64]{0,1:T(8,128)(2,1)}, u32[]{:S(2)}) copy-start(bf16[2048,64]{0,1:T(8,128)(2,1)} %param.29) | copy-start | bytes 786436
  134.9 1.6 %copy-start.4 = (f32[128,64]{1,0:T(8,128)S(1)}, f32[128,64]{1,0:T(8,128)}, u32[]{:S(2)}) copy-start(f32[128,64]{1,0:T(8,128)} %get-tuple-element.12) | copy-start | bytes 98308
  136.5 0.8 copy-start.3
  138.0 1.9 %copy-start.1 = (bf16[1,2048,128]{2,1,0:T(8,128)(2,1)S(1)}, bf16[1,2048,128]{2,1,0:T(8,128)(2,1)}, u32[]{:S(2)}) copy-start(bf16[1,2048,128]{2,1,0:T(8,128)(2,1)} %get-tuple-element.22) | copy-start | bytes 1572868
  140.0 1.2 copy-start
  141.2 0.8 copy-start.5

commit v2 on v1

--- a/solution.py
+++ b/solution.py
@@ -14,6 +14,7 @@
 SHIFT = 3
 COLS = 128
 CAP = 16
+FULL = 67_043_328
 
 
 def dot(a, b, ca, cb):
@@ -128,24 +129,24 @@
 
 def kernel(
     ns,
-    cot,
-    norm,
-    irms,
-    gain,
-    routes,
-    prob,
-    gate_w,
-    up_w,
-    down_w,
-    rec_in,
-    rec_gate,
-    in_gate,
-    decay_w,
-    extra,
-    out_m,
-    g_gate,
-    g_up,
-    g_down,
+    cot_h,
+    norm_h,
+    irms_h,
+    gain_h,
+    routes_h,
+    prob_h,
+    gate_h,
+    up_h,
+    down_h,
+    rec_in_h,
+    rec_gate_h,
+    in_gate_h,
+    decay_h,
+    extra_h,
+    out_h,
+    g_gate_h,
+    g_up_h,
+    g_down_h,
     g_out,
     g_rec,
     g_dec,
@@ -168,8 +169,6 @@
     arrived,
     dn,
     d_mix,
-    scan_a,
-    scan_b,
     rows_f,
     lead,
     leads,
@@ -180,6 +179,24 @@
     gw_pair,
     gw_chip,
     gw_in,
+    down_w,
+    g_gate,
+    g_up,
+    g_down,
+    cot,
+    norm,
+    irms,
+    gain,
+    routes,
+    prob,
+    rec_in,
+    rec_gate,
+    in_gate,
+    decay_w,
+    extra,
+    out_m,
+    w_r,
+    g_s,
     z_s,
     z_r,
     ag_s,
@@ -221,6 +238,13 @@
     steps = [d for d in steps] + [-4] + [4, 5, -5, 6, -6, 7, -7, 8]
     others = [(0, 1)] + [(d, c) for d in steps for c in (0, 1)]
 
+    def far_first(pairs):
+        near_ones = [p for p in pairs if place(p[0]) < near]
+        return near_ones[::-1] + [p for p in pairs if place(p[0]) >= near][::-1]
+
+    def place(d):
+        return (SHIFT - d) % nz
+
     def other(d, c):
         if d == 0:
             return z * 2 + (1 - core)
@@ -236,42 +260,74 @@
             barrier, inc=1, device_id=to_y(lax.rem(y + v, SIDE)), device_id_type=MESH
         )
 
+    moves = (
+        (routes_h, routes),
+        (prob_h, prob),
+        (norm_h, norm),
+        (cot_h, cot),
+        (rec_gate_h, rec_gate),
+        (in_gate_h, in_gate),
+        (rec_in_h, rec_in),
+        (decay_h, decay_w),
+        (extra_h, extra),
+        (gate_h.at[0], wide.at[:, :COLS]),
+        (up_h.at[0], wide.at[:, COLS:]),
+        (down_h.at[0], down_w),
+        (irms_h, irms),
+        (gain_h, gain),
+        (out_h, out_m),
+    )
+    moves = [pltpu.make_async_copy(a, b, w_r.at[k]) for k, (a, b) in enumerate(moves)]
+    for copy in moves:
+        copy.start()
+
+    def have(first, last):
+        for copy in moves[first:last]:
+            copy.wait()
+
     mine = pl.ds(pl.multiple_of(tp * COLS, COLS), COLS)
-    lane = lax.broadcasted_iota(jnp.int32, (tokens, ns), 1)
-    chosen = [routes[:, k : k + 1] for k in (0, 1)]
-    member = [(e == lane).astype(F32) for e in chosen]
+    def eye(n):
+        return lax.broadcasted_iota(jnp.int32, (n, n), 0) == lax.broadcasted_iota(
+            jnp.int32, (n, n), 1
+        )
+
+    square = eye(tokens)
+
+    def upright(row):
+        return jnp.sum(jnp.where(square, row, 0.0), axis=1, keepdims=True)
+
+    have(0, 4)
+    expert_id = lax.broadcasted_iota(jnp.int32, (ns, tokens), 0)
+    chosen = [routes[k : k + 1, :] for k in (0, 1)]
+    member = [(e == expert_id).astype(F32) for e in chosen]
     earlier = (
-        lax.broadcasted_iota(jnp.int32, (tokens, tokens), 1)
-        < lax.broadcasted_iota(jnp.int32, (tokens, tokens), 0)
+        lax.broadcasted_iota(jnp.int32, (tokens, tokens), 0)
+        < lax.broadcasted_iota(jnp.int32, (tokens, tokens), 1)
     ).astype(BF16)
-    before = dot(earlier, (member[0] + member[1]).astype(BF16), 1, 0)
-    slot = lax.broadcasted_iota(jnp.int32, (tokens, ns * CAP), 1).astype(F32)
-    at = [
-        slot
-        == (e.astype(F32) * CAP + jnp.sum(m * before, axis=1, keepdims=True))
+    before = dot((member[0] + member[1]).astype(BF16), earlier, 1, 0)
+    slot = lax.broadcasted_iota(jnp.int32, (ns * CAP, tokens), 0).astype(F32)
+    one = [
+        (slot == (e.astype(F32) * CAP + jnp.sum(m * before, axis=0, keepdims=True))).astype(F32)
         for e, m in zip(chosen, member)
     ]
-    one = [a.astype(F32) for a in at]
     both = (one[0] + one[1]).astype(BF16)
     picked[...] = both
     own_cot = cot[:, mine].astype(F32)
-    packed[0] = dot(both, norm[:, mine], 0, 0).astype(BF16)
+    packed[0] = dot(both, norm[:, mine], 1, 0).astype(BF16)
     packed[1] = (
-        dot(one[0].astype(BF16), (prob[:, 0:1] * own_cot).astype(BF16), 0, 0)
-        + dot(one[1].astype(BF16), (prob[:, 1:2] * own_cot).astype(BF16), 0, 0)
+        dot(one[0].astype(BF16), (upright(prob[0:1, :]) * own_cot).astype(BF16), 1, 0)
+        + dot(one[1].astype(BF16), (upright(prob[1:2, :]) * own_cot).astype(BF16), 1, 0)
     ).astype(BF16)
 
-    pl.semaphore_wait(barrier, len(others) + 4)
+    with jax.named_scope("barrier"):
+        pl.semaphore_wait(barrier, len(others) + 4)
 
     own_x = pl.ds(pl.multiple_of(x * COLS, COLS), COLS)
-
-    def place(d):
-        return lax.rem(SHIFT - d + 2 * nz, nz) if not isinstance(d, int) else (SHIFT - d) % nz
 
     def rows_at(pos, c):
         return pl.ds(pl.multiple_of((pos * 2 + c) * CAP, CAP), CAP)
 
-    for d, c in others:
+    for d, c in far_first(others):
         target = other(d, c)
         k = 0 if place(d) < near else 1
         send(
@@ -287,54 +343,57 @@
         z_r.at[0],
     ).start()
 
-    channels = extra.shape[1]
-    retain = jax.nn.sigmoid(rec_gate[...].astype(F32))
-    admit = jax.nn.sigmoid(in_gate[...].astype(F32))
-    signal = rec_in[...].astype(F32)
-    speed = -8.0 * softplus(-decay_w[...])
-    log_keep = retain * speed + extra[...]
-    keep = jnp.exp(log_keep)
-    scale_in = jnp.sqrt(-expm1(2.0 * log_keep))
-    pad = 64
-    scan_a[pl.ds(0, pad), :] = jnp.ones((pad, channels), F32)
-    scan_a[pl.ds(pad + tokens, pad), :] = jnp.ones((pad, channels), F32)
-    scan_b[pl.ds(0, pad), :] = jnp.zeros((pad, channels), F32)
-    scan_b[pl.ds(pad + tokens, pad), :] = jnp.zeros((pad, channels), F32)
-    body = pl.ds(pad, tokens)
+    channels = extra.shape[0]
+    corner = eye(channels)
+
+    def lying(column):
+        return jnp.sum(jnp.where(corner, column, 0.0), axis=0, keepdims=True)
+
+    def standing(row):
+        return jnp.sum(jnp.where(corner, row, 0.0), axis=1, keepdims=True)
+
+    token = lax.broadcasted_iota(jnp.int32, (channels, tokens), 1)
+
+    def moved(v, step, fill):
+        inside = token >= step if step > 0 else token < tokens + step
+        return jnp.where(inside, pltpu.roll(v, step % tokens, 1), fill)
 
     def scan(a, b, sign):
         step = 1
         while step < tokens:
-            scan_a[body, :] = a
-            scan_b[body, :] = b
-            moved = pl.ds(pad - sign * step, tokens)
-            b = a * scan_b[moved, :] + b
-            a = a * scan_a[moved, :]
+            b = a * moved(b, sign * step, 0.0) + b
+            a = a * moved(a, sign * step, 1.0)
             step *= 2
         return a, b
 
-    keep_cum, state_loc = scan(keep, scale_in * admit * signal, 1)
-    lead[...] = jnp.concatenate(
-        [keep_cum[tokens - 1 :, :], state_loc[tokens - 1 :, :]], axis=1
-    )
-    leads[sp] = lead[...]
-    for d, c in others:
-        send(lead, leads.at[sp], lead_s, lead_r, to_sp(other(d, c)))
-    scan_a[body, :] = keep
-    keep_next = scan_a[pl.ds(pad + 1, tokens), :]
-    rows_f[0] = keep_cum
-    rows_f[1] = state_loc
-    rows_f[2] = keep
-    rows_f[3] = keep_next
-    rows_f[4] = scale_in * admit
-    rows_f[5] = scale_in * signal * admit * (1.0 - admit)
-    rows_f[6] = admit * signal * keep * keep / scale_in
-    rows_f[7] = speed * retain * (1.0 - retain)
-    wide[:, :COLS] = gate_w[0]
-    wide[:, COLS:] = up_w[0]
+    with jax.named_scope("recur"):
+        have(4, 9)
+        retain = jax.nn.sigmoid(rec_gate[...].astype(F32))
+        admit = jax.nn.sigmoid(in_gate[...].astype(F32))
+        signal = rec_in[...].astype(F32)
+        speed = standing(-8.0 * softplus(-decay_w[...]))
+        log_keep = retain * speed + extra[...]
+        keep = jnp.exp(log_keep)
+        scale_in = jnp.sqrt(-expm1(2.0 * log_keep))
+        keep_cum, state_loc = scan(keep, scale_in * admit * signal, 1)
+        lead[...] = jnp.concatenate(
+            [lying(keep_cum[:, tokens - 1 :]), lying(state_loc[:, tokens - 1 :])], axis=1
+        )
+        leads[sp] = lead[...]
+        for d, c in others:
+            send(lead, leads.at[sp], lead_s, lead_r, to_sp(other(d, c)))
+        rows_f[0] = keep_cum
+        rows_f[1] = state_loc
+        rows_f[2] = keep
+        rows_f[3] = moved(keep, -1, 1.0)
+        rows_f[4] = scale_in * admit
+        rows_f[5] = scale_in * signal * admit * (1.0 - admit)
+        rows_f[6] = admit * signal * keep * keep / scale_in
+        rows_f[7] = speed * retain * (1.0 - retain)
 
     def z_arrived(k):
-        take(rows.at[:, y, pl.ds(k * chunk, chunk), own_x], z_r.at[k])
+        with jax.named_scope(f"z_arrived{k}"):
+            take(rows.at[:, y, pl.ds(k * chunk, chunk), own_x], z_r.at[k])
 
     def gathers(k):
         base, half_rows = k * chunk, chunk // 2
@@ -366,7 +425,7 @@
         d_act = jnp.zeros((chunk, COLS), F32)
         for j in range(SIDE):
             hidden += dot(rows[0, j, span, :], wide[j * deep : (j + 1) * deep, :], 1, 0)
-            d_act += dot(rows[1, j, span, :], down_w[0, :, j * deep : (j + 1) * deep], 1, 1)
+            d_act += dot(rows[1, j, span, :], down_w[:, j * deep : (j + 1) * deep], 1, 1)
         gate_pre, up_pre = hidden[:, :COLS], hidden[:, COLS:]
         sigma = jax.nn.sigmoid(gate_pre)
         swish = gate_pre * sigma
@@ -433,7 +492,7 @@
                     BF16
                 )
         dst = arrived.at[pl.ds(pl.multiple_of(sp * CAP, CAP), CAP), :]
-        for d, c in others:
+        for d, c in others[::-1]:
             pos = place(-d)
             if (pos < near) != (k == 0):
                 continue
@@ -442,9 +501,10 @@
         if k == 0:
             pltpu.make_async_copy(back.at[rows_at(SHIFT, core), :], dst, back_r).start()
 
-    def each(rings, name):
-        for ring in rings:
-            getattr(ring, name)()
+    def each(rings, name, label=""):
+        with jax.named_scope(label + name):
+            for ring in rings:
+                getattr(ring, name)()
 
     a0, b0 = gathers(0)
     a1, b1 = gathers(1)
@@ -452,46 +512,58 @@
     r1, q1 = scatters(1)
 
     z_arrived(0)
-    each(a0, "first")
-    each(a0, "relay")
-    each(a0, "last")
-    each(b0, "first")
+    each(a0, "first", "a0_")
+    each(a0, "relay", "a0_")
+    each(a0, "last", "a0_")
+    each(b0, "first", "b0_")
     z_arrived(1)
-    each(a1, "first")
-    each(b0, "relay")
-    each(a1, "relay")
-    each(b0, "last")
-    each(a1, "last")
-    each(b1, "first")
-    expert(0)
-    each(r0, "first")
-    each(b1, "relay")
-    each(r0, "relay")
-    each(r0, "last")
+    each(a1, "first", "a1_")
+    each(b0, "relay", "b0_")
+    each(a1, "relay", "a1_")
+    each(b0, "last", "b0_")
+    each(a1, "last", "a1_")
+    each(b1, "first", "b1_")
+    have(9, 15)
+    with jax.named_scope("expert0"):
+        expert(0)
+    each(r0, "first", "r0_")
+    each(b1, "relay", "b1_")
+    each(r0, "relay", "r0_")
+    each(r0, "last", "r0_")
     between(0, r0)
-    each(q0, "first")
-    each(b1, "last")
-    expert(1)
-    each(r1, "first")
-    each(q0, "relay")
-    each(q0, "last")
+    each(q0, "first", "q0_")
+    each(b1, "last", "b1_")
+    with jax.named_scope("expert1"):
+        expert(1)
+    each(r1, "first", "r1_")
+    each(q0, "relay", "q0_")
+    each(q0, "last", "q0_")
     give_back(0, q0)
-    each(r1, "relay")
-    each(r1, "last")
+    each(r1, "relay", "r1_")
+    each(r1, "last", "r1_")
     between(1, r1)
-    each(q1, "first")
-    each(q1, "relay")
-    each(q1, "last")
+    each(q1, "first", "q1_")
+    each(q1, "relay", "q1_")
+    each(q1, "last", "q1_")
     give_back(1, q1)
 
-    deep = rows.shape[3]
-    for j in range(SIDE):
-        grads = dot(rows[0, j], d_wide[...], 0, 0).astype(BF16)
-        g_gate[0, j * deep : (j + 1) * deep, :] = grads[:, :COLS]
-        g_up[0, j * deep : (j + 1) * deep, :] = grads[:, COLS:]
-        g_down[0, :, j * deep : (j + 1) * deep] = dot(act[...], rows[1, j], 0, 0).astype(BF16)
-
-    take(leads.at[pl.ds(0, ns - 1)], lead_r)
+    with jax.named_scope("grads"):
+        deep = rows.shape[3]
+        for j in range(SIDE):
+            grads = dot(rows[0, j], d_wide[...], 0, 0).astype(BF16)
+            g_gate[j * deep : (j + 1) * deep, :] = grads[:, :COLS]
+            g_up[j * deep : (j + 1) * deep, :] = grads[:, COLS:]
+            g_down[:, j * deep : (j + 1) * deep] = dot(act[...], rows[1, j], 0, 0).astype(BF16)
+        stored = (
+            pltpu.make_async_copy(g_gate, g_gate_h.at[0], g_s.at[0]),
+            pltpu.make_async_copy(g_up, g_up_h.at[0], g_s.at[1]),
+            pltpu.make_async_copy(g_down, g_down_h.at[0], g_s.at[2]),
+        )
+        for copy in stored:
+            copy.start()
+
+    with jax.named_scope("lead_wait"):
+        take(leads.at[pl.ds(0, ns - 1)], lead_r)
     state_in = jnp.zeros((1, channels), F32)
     for i in range(ns):
         v = leads[i]
@@ -500,104 +572,139 @@
     for i in range(ns):
         coef[i] = jnp.where(i > sp, run, 0.0)
         run = jnp.where(i > sp, run * leads[i][:, :channels], run)
+    state_in = standing(state_in)
     state = rows_f[1] + rows_f[0] * state_in
-    scan_b[body, :] = state
-    first_row = lax.broadcasted_iota(jnp.int32, (tokens, channels), 0) == 0
-    state_prev = jnp.where(first_row, state_in, scan_b[pl.ds(pad - 1, tokens), :])
-    rows_f[6] = (state_prev * rows_f[2] - rows_f[6]) * rows_f[7]
+    rows_f[6] = (moved(state, 1, state_in) * rows_f[2] - rows_f[6]) * rows_f[7]
     hidden = state.astype(BF16)
 
-    take(arrived, back_r)
-    dn[y, :, own_x] = dot(picked[...], arrived[...], 1, 0).astype(BF16)
+    with jax.named_scope("back_wait"):
+        take(arrived, back_r)
+    dn[y, :, own_x] = dot(picked[...], arrived[...], 0, 0).astype(BF16)
     half = tokens // 2
-    quarter = tokens // 4
-
-    def at_x(i):
-        return pl.ds(pl.multiple_of(i * COLS, COLS), COLS)
-
-    def piece(start, h):
-        return pl.ds(start, half) if h is None else pl.ds(start + h * quarter, quarter)
-
-    shapes = (
-        (lambda i, h: dn.at[y, piece(0, h), at_x(i)], x, to_x),
-        (lambda i, h: dn.at[i, piece(half, h), own_x], y, to_y),
-        (lambda i, h: dn.at[i, piece(0, h), :], y, to_y),
-        (lambda i, h: dn.at[:, piece(half, h), at_x(i)], x, to_x),
-    )
-    dg = [Gather(b, i, to, dn_s.at[n], dn_r.at[n]) for n, (b, i, to) in enumerate(shapes)]
-    for pair in (dg[:2], dg[2:]):
-        each(pair, "first")
-        each(pair, "relay")
-        each(pair, "last")
-
-    eye = lax.broadcasted_iota(jnp.int32, (tokens, tokens), 0) == lax.broadcasted_iota(
-        jnp.int32, (tokens, tokens), 1
-    )
-    inv_rms = jnp.sum(jnp.where(eye, irms[...], 0.0), axis=1, keepdims=True)
-    stat = jnp.zeros((tokens, 1), F32)
-    for j in range(SIDE):
-        cols = pl.ds(j * deep, deep)
-        g = gain[:, cols]
-        stat += jnp.sum(
-            (g * dn[j].astype(F32)) * (norm[:, cols].astype(F32) / g), axis=1, keepdims=True
-        )
-    stat = stat / norm.shape[1]
-    for j in range(SIDE):
-        cols = pl.ds(j * deep, deep)
-        g = gain[:, cols]
-        mix = cot[:, cols].astype(F32) + inv_rms * (
-            g * dn[j].astype(F32) - (norm[:, cols].astype(F32) / g) * stat
-        )
-        d_mix[:, cols] = mix.astype(BF16)
-
-    d_state = dot(d_mix[...], out_m[...], 1, 0)
-    tail, grad_loc = scan(rows_f[3], d_state, -1)
-    first_grad = rows_f[2][:1, :] * grad_loc[:1, :]
-    trail[...] = jnp.concatenate([first_grad, first_grad], axis=1)
-    trails[sp] = trail[...]
-    for d, c in others:
-        send(trail, trails.at[sp], trail_s, trail_r, to_sp(other(d, c)))
-
-    g_rows = g_out.shape[0]
-    gw = dot(d_mix[...], hidden, 0, 0).astype(BF16)
-    for n in range(ns):
-        low = n * g_rows
-        gw_all[n % 2, n // 2] = jnp.concatenate(
-            [gw[low : low + g_rows // 2, :], gw[low + g_rows // 2 : low + g_rows, :]], axis=1
-        )
+
+    def spot(n, i, j):
+        return dn.at[j, pl.ds(n * half, half), pl.ds(pl.multiple_of(i * COLS, COLS), COLS)]
+
+    def spread(n, i, j, along_x, slot):
+        ref = spot(n, i, j)
+        for v in (2, 1, 3):
+            target = to_x(lax.rem(x + v, SIDE)) if along_x else to_y(lax.rem(y + v, SIDE))
+            send(ref, ref, dn_s.at[n, slot, v - 1], dn_r.at[n, slot, v - 1], target)
+
+    def back_by(p, v):
+        return lax.rem(p + SIDE - v, SIDE)
+
+    for n in (0, 1):
+        spread(n, x, y, n == 0, 0)
+    for n in (0, 1):
+        spread(n, x, y, n == 1, 1)
+    with jax.named_scope("dn_first"):
+        for v in (1, 3, 2):
+            for n in (0, 1):
+                i, j = (back_by(x, v), y) if n == 0 else (x, back_by(y, v))
+                take(spot(n, i, j), dn_r.at[n, 0, v - 1])
+                spread(n, i, j, n == 1, 1 + v)
+    with jax.named_scope("dn_last"):
+        for v in (0, 1, 3, 2):
+            for w in (1, 3, 2):
+                for n in (0, 1):
+                    i, j = (
+                        (back_by(x, v), back_by(y, w)) if n == 0 else (back_by(x, w), back_by(y, v))
+                    )
+                    take(spot(n, i, j), dn_r.at[n, 1 + v, w - 1])
+
+    with jax.named_scope("mix"):
+        inv_rms = upright(irms[...])
+        stat = jnp.zeros((tokens, 1), F32)
+        for j in range(SIDE):
+            cols = pl.ds(j * deep, deep)
+            g = gain[:, cols]
+            stat += jnp.sum(
+                (g * dn[j].astype(F32)) * (norm[:, cols].astype(F32) / g), axis=1, keepdims=True
+            )
+        stat = stat / norm.shape[1]
+        for j in range(SIDE):
+            cols = pl.ds(j * deep, deep)
+            g = gain[:, cols]
+            mix = cot[:, cols].astype(F32) + inv_rms * (
+                g * dn[j].astype(F32) - (norm[:, cols].astype(F32) / g) * stat
+            )
+            d_mix[:, cols] = mix.astype(BF16)
+
+    with jax.named_scope("trail"):
+        d_state = dot(out_m[...], d_mix[...], 1, 1)
+        tail, grad_loc = scan(rows_f[3], d_state, -1)
+        first_grad = lying(rows_f[2][:, :1] * grad_loc[:, :1])
+        trail[...] = jnp.concatenate([first_grad, first_grad], axis=1)
+        trails[sp] = trail[...]
+        for d, c in others:
+            send(trail, trails.at[sp], trail_s, trail_r, to_sp(other(d, c)))
+
+    with jax.named_scope("gw_dot"):
+        wide_piece = 2 * g_out.shape[0]
+        gw = dot(hidden, d_mix[...], 1, 0)
+        for n in range(nz):
+            band = gw[:, n * wide_piece : (n + 1) * wide_piece]
+            top, low = band[: channels // 2, :], band[channels // 2 :, :]
+            cut = g_out.shape[0]
+            gw_all[0, n] = jnp.concatenate([top[:, :cut], low[:, :cut]], axis=1).astype(BF16)
+            gw_all[1, n] = jnp.concatenate([top[:, cut:], low[:, cut:]], axis=1).astype(BF16)
+
     send(gw_all.at[1 - core], gw_pair, pair_s, pair_r, to_sp(z * 2 + 1 - core))
-    take(trails.at[pl.ds(0, ns - 1)], trail_r)
+    with jax.named_scope("pair_wait"):
+        take(gw_pair, pair_r)
+    gw_chip[...] = (gw_all[core].astype(F32) + gw_pair[...].astype(F32)).astype(BF16)
+    for d in steps[::-1]:
+        zz = lax.rem(z + d + nz, nz)
+        send(gw_chip.at[zz], gw_in.at[z], gw_s, gw_r, to_sp(zz * 2 + core))
+    pltpu.make_async_copy(gw_chip.at[z], gw_in.at[z], gw_r).start()
+    with jax.named_scope("trail_wait"):
+        take(trails.at[pl.ds(0, ns - 1)], trail_r)
     entering = jnp.zeros((1, channels), F32)
     for i in range(ns):
         entering += coef[i] * trails[i][:, :channels]
-    total = grad_loc + tail * entering
-    take(gw_pair, pair_r)
-    gw_chip[...] = (gw_all[core].astype(F32) + gw_pair[...].astype(F32)).astype(BF16)
-    for d in steps:
-        zz = lax.rem(z + d + nz, nz)
-        send(gw_chip.at[zz], gw_in.at[z], gw_s, gw_r, to_sp(zz * 2 + core))
-    pltpu.make_async_copy(gw_chip.at[z], gw_in.at[z], gw_r).start()
+    total = grad_loc + tail * standing(entering)
     g_rec[...] = total * rows_f[4]
     g_in[...] = total * rows_f[5]
     g_dec[...] = total * rows_f[6]
-    take(gw_in, gw_r)
-    acc = jnp.zeros((g_rows // 2, 2 * channels), F32)
+    with jax.named_scope("gw_wait"):
+        take(gw_in, gw_r)
+    acc = jnp.zeros(gw_in.shape[1:], F32)
     for i in range(nz):
         acc += gw_in[i].astype(F32)
-    g_out[: g_rows // 2, :] = acc[:, :channels]
-    g_out[g_rows // 2 :, :] = acc[:, channels:]
-
+    cut = g_out.shape[0]
+    g_out[...] = jnp.concatenate([acc[:, :cut], acc[:, cut:]], axis=0).T
+
+    for copy in stored:
+        copy.wait()
     block = ns // 2 * CAP
     take(packed.at[:, pl.ds(0, block - CAP), :], z_s.at[0])
     take(packed.at[:, pl.ds(0, block), :], z_s.at[1])
-    for ring in a0 + b0 + a1 + b1 + list(r0) + list(q0) + list(r1) + list(q1) + dg:
+    for ring in a0 + b0 + a1 + b1 + list(r0) + list(q0) + list(r1) + list(q1):
         ring.sent()
+    for n in (0, 1):
+        for slot in range(5):
+            for v in range(3):
+                take(spot(n, x, y), dn_s.at[n, slot, v])
     take(back.at[pl.ds(0, block - CAP), :], back_s.at[0])
     take(back.at[pl.ds(0, block), :], back_s.at[1])
     take(leads.at[pl.ds(0, ns - 1)], lead_s)
     take(trails.at[pl.ds(0, ns - 1)], trail_s)
     take(gw_pair, pair_s)
     take(gw_in.at[pl.ds(0, nz - 1)], gw_s)
+
+
+def finish(count, *refs):
+    held, came, left = refs[2 * count : 3 * count], refs[-2], refs[-1]
+    into = [pltpu.make_async_copy(refs[n], held[n], came.at[n]) for n in range(count)]
+    out = [pltpu.make_async_copy(held[n], refs[count + n], left.at[n]) for n in range(count)]
+    for copy in into:
+        copy.start()
+    for first, second in zip(into, out):
+        first.wait()
+        second.start()
+    for copy in out:
+        copy.wait()
 
 
 def shards(
@@ -629,20 +736,21 @@
         normed,
         inverse_root_mean_square.reshape(1, tokens),
         expert_norm_scale.reshape(1, features),
-        routes,
-        route_probability_weight,
+        routes.T,
+        route_probability_weight.T,
         gate_weight,
         up_weight,
         down_weight,
-        recurrence_input,
-        recurrence_gate_logits,
-        input_gate_logits,
+        recurrence_input.T,
+        recurrence_gate_logits.T,
+        input_gate_logits.T,
         channel_decay_weight.reshape(1, channels),
-        extra_log_decay,
-        output_matrix,
+        extra_log_decay.T,
+        output_matrix.T,
     )
-    f32_rows = jax.ShapeDtypeStruct((tokens, channels), F32)
-    return pl.pallas_call(
+    f32_rows = jax.ShapeDtypeStruct((channels, tokens), F32)
+    vm, hbm = pl.BlockSpec(memory_space=pltpu.VMEM), pl.BlockSpec(memory_space=pl.ANY)
+    results = pl.pallas_call(
         functools.partial(kernel, ns),
         out_shape=(
             jax.ShapeDtypeStruct(gate_weight.shape, BF16),
@@ -653,11 +761,11 @@
             f32_rows,
             f32_rows,
         ),
-        in_specs=[pl.BlockSpec(memory_space=pltpu.VMEM)] * len(args),
-        out_specs=[pl.BlockSpec(memory_space=pltpu.VMEM)] * 7,
+        in_specs=[hbm] * len(args),
+        out_specs=[hbm] * 3 + [vm] * 4,
         scratch_shapes=[
             vmem((2, slots, COLS), BF16),
-            vmem((tokens, slots), BF16),
+            vmem((slots, tokens), BF16),
             vmem((2, SIDE, slots, wide), BF16),
             vmem((features, 2 * COLS), BF16),
             vmem((slots, 2 * COLS), BF16),
@@ -674,9 +782,7 @@
             vmem((slots, COLS), BF16),
             vmem((SIDE, tokens, wide), BF16),
             vmem((tokens, features), BF16),
-            vmem((tokens + 128, channels), F32),
-            vmem((tokens + 128, channels), F32),
-            vmem((8, tokens, channels), F32),
+            vmem((8, channels, tokens), F32),
             vmem((1, 2 * channels), F32),
             vmem((ns, 1, 2 * channels), F32),
             vmem((1, 2 * channels), F32),
@@ -686,14 +792,22 @@
             vmem((ns // 2, features // ns // 2, 2 * channels), BF16),
             vmem((ns // 2, features // ns // 2, 2 * channels), BF16),
             vmem((ns // 2, features // ns // 2, 2 * channels), BF16),
+            vmem((COLS, features), BF16),
+            vmem((features, COLS), BF16),
+            vmem((features, COLS), BF16),
+            vmem((COLS, features), BF16),
+            *(vmem(args[n].shape, args[n].dtype) for n in (0, 1, 2, 3, 4, 5)),
+            *(vmem(a.shape, a.dtype) for a in args[9:]),
+            dma((len(args),)),
+            dma((3,)),
             dma((2,)),
             dma((2,)),
             dma((8, 4)),
             dma((8, 4)),
             dma((8, 6)),
             dma((8, 6)),
-            dma((4, 4)),
-            dma((4, 4)),
+            dma((2, 5, 3)),
+            dma((2, 5, 3)),
             dma((2,)),
             dma,
             dma,
@@ -706,9 +820,19 @@
             dma,
         ],
         compiler_params=pltpu.CompilerParams(
-            collective_id=0, has_side_effects=True, vmem_limit_bytes=60 * 1024 * 1024
+            collective_id=0, has_side_effects=True, vmem_limit_bytes=FULL
         ),
     )(*args)
+    g_gate, g_up, g_down, g_out, g_rec, g_dec, g_in = pl.pallas_call(
+        functools.partial(finish, len(results)),
+        out_shape=tuple(jax.ShapeDtypeStruct(r.shape, r.dtype) for r in results),
+        in_specs=[hbm] * len(results),
+        out_specs=[hbm] * len(results),
+        scratch_shapes=[vmem(r.shape, r.dtype) for r in results]
+        + [dma((len(results),)), dma((len(results),))],
+        compiler_params=pltpu.CompilerParams(vmem_limit_bytes=FULL),
+    )(*results)
+    return g_gate, g_up, g_down, g_out, g_rec.T, g_dec.T, g_in.T
 
 
 def solution(mesh):

time: 143 us -> 115 us (0.80)
  local copies, waits for them, and re-layouts: 17.3 us -> 0 us
  Pallas kernels: 125 us -> 114 us
    unnamed x23 -> x0, local copies, waits for them, and re-layouts: 14.4 us -> none
    pallas_call x1, Pallas kernels: 125 us -> 112 us  [shards(): pl.pallas_call(functools.partial(kernel, ns), out_shape=(jax.ShapeDtypeSt...]
    pallas_call x3 -> x0, local copies, waits for them, and re-layouts: 2.96 us -> none  [shards(): pl.pallas_call(functools.partial(kernel, ns), out_shape=(jax.ShapeDtypeSt...]
    pallas_call x0 -> x1, Pallas kernels: none -> 2.33 us  [shards(): pl.pallas_call(functools.partial(finish, len(results)), out_shape=tuple((...]
where the time goes in v2:
time: 115 us
  Pallas kernels  114 us (99%)
    pallas_call x1, Pallas kernels, shards(): pl.pallas_call(functools.partial(kernel, ns), out_shape=(jax.ShapeDtypeSt...  112 us
    pallas_call x1, Pallas kernels, shards(): pl.pallas_call(functools.partial(finish, len(results)), out_shape=tuple((...  2.33 us

profile of v2, /device:TPU:1, one launch (start us, length us, event | category | flops | bytes accessed | tf_op | source)
XLA Modules:
  0.0 115.0 jit_solution(5972161185978395797)
XLA Ops:
  0.6 112.1 %shard_map.198 = (bf16[1,2048,128]{2,1,0:T(8,128)(2,1)}, bf16[1,2048,128]{2,1,0:T(8,128)(2,1)}, bf16[1,128,2048]{2,1,0:T(8,128)(2,1)}, f32[64,64]{1,0:T(8,128)},...) custom-call(bf16[128,2048]{1,0:T(8,128)(2,1)} %cot_h.1, bf16[128,2048]{1,0:T(8,128)(2,1)} %norm_h.1, ...), custom_call_target="tpu_custom_call" | custom-call | tf_op jit(solution)/shard_map/pallas_call | solution.py:753
  112.7 2.3 %shard_map.199 = (bf16[1,2048,128]{2,1,0:T(8,128)(2,1)}, bf16[1,2048,128]{2,1,0:T(8,128)(2,1)}, bf16[1,128,2048]{2,1,0:T(8,128)(2,1)}, f32[64,64]{1,0:T(8,128)},...) custom-call(bf16[1,2048,128]{2,1,0:T(8,128)(2,1)} %get-tuple-element.21.refs_0_, ...), custom_call_target="tpu_custom_call" | custom-call | tf_op jit(solution)/shard_map/pallas_call | solution.py:826

commit v3 on v2

--- a/solution.py
+++ b/solution.py
@@ -11,8 +11,10 @@
 F32 = jnp.float32
 BF16 = jnp.bfloat16
 SIDE = 4
-SHIFT = 3
+CHUNKS = (4, 6, 4, 2)
 COLS = 128
+ORDER = (('begin', 0), ('near', 0), ('relay', 0, 0), ('begin', 1), ('across', 0), ('relay', 0, 2), ('relay', 0, 1), ('near', 1), ('relay', 1, 0), ('relay', 0, 3), ('begin', 2), ('across', 1), ('relay', 1, 2), ('relay', 1, 1), ('begin', 3), ('expert', 0), ('near', 2), ('relay', 2, 0), ('relay', 1, 3), ('near', 3), ('relay', 3, 0), ('mid', 0), ('across', 2), ('relay', 2, 2), ('relay', 2, 1), ('expert', 1), ('across', 3), ('relay', 3, 2), ('relay', 3, 1), ('turn', 0), ('relay', 2, 3), ('mid', 1), ('relay', 3, 3), ('expert', 2), ('give', 0), ('turn', 1), ('expert', 3), ('mid', 2), ('give', 1), ('mid', 3), ('turn', 2), ('turn', 3), ('give', 2), ('give', 3))
+FIRST_EXPERT = [step for step, *_ in ORDER].index("expert")
 CAP = 16
 FULL = 67_043_328
 
@@ -36,77 +38,107 @@
     ).start()
 
 
-class Gather:
-    def __init__(self, block, i, axis_to, ss, rs):
+class Flow:
+    def __init__(self, piece, bulk, p, q, to_p, to_q, ss, rs):
+        self.piece, self.bulk, self.p, self.q, self.to_p, self.to_q, self.ss, self.rs = (
+            piece, bulk, p, q, to_p, to_q, ss, rs,
+        )
+        self.from_p = [p] + [lax.rem(p + SIDE - v, SIDE) for v in (1, 3, 2)]
+
+    def along_p(self, ref, v, k):
+        send(ref, ref, self.ss, self.rs.at[k], self.to_p(lax.rem(self.p + v, SIDE)))
+
+    def along_q(self, ref, v, k):
+        send(ref, ref, self.ss, self.rs.at[k], self.to_q(lax.rem(self.q + v, SIDE)))
+
+    def mine(self, m, half=None):
+        return self.piece(self.from_p[m], self.q, half)
+
+    def other(self, m, v, half=None):
+        return self.piece(self.from_p[m], lax.rem(self.q + SIDE - v, SIDE), half)
+
+    def cross(self, m):
+        self.along_q(self.mine(m), 1, 3 + m)
+        self.along_q(self.mine(m), 3, 3 + m)
+
+    def start(self):
+        self.along_p(self.mine(0), 1, 0)
+        self.along_p(self.mine(0), 3, 0)
+        self.cross(0)
+
+    def near(self):
+        take(self.bulk(2), self.rs.at[0])
+        self.along_p(self.mine(1, 0), 1, 1)
+        self.along_p(self.mine(2, 1), 3, 1)
+        self.cross(1)
+        self.cross(2)
+
+    def across(self):
+        take(self.bulk(1), self.rs.at[1])
+        self.cross(3)
+
+    def relay(self, m):
+        take(self.bulk(2), self.rs.at[3 + m])
+        self.along_q(self.other(m, 1, 0), 1, 2)
+        self.along_q(self.other(m, 3, 1), 3, 2)
+
+    def last(self):
+        take(self.bulk(SIDE), self.rs.at[2])
+
+
+class Scatter:
+    def __init__(self, block, i, axis_to, ss, rs, part, came, parts, all_came):
         self.block, self.i, self.to, self.ss, self.rs = block, i, axis_to, ss, rs
+        self.part, self.came, self.parts, self.all_came = part, came, parts, all_came
         self.up, self.down, self.far = lax.rem(i + 1, 4), lax.rem(i + 3, 4), lax.rem(i + 2, 4)
 
-    def go(self, src, half, target, k):
-        ref = self.block(src, half)
-        send(ref, ref, self.ss.at[k], self.rs.at[k], target)
-
-    def first(self):
-        self.go(self.i, None, self.to(self.up), 0)
-        self.go(self.i, None, self.to(self.down), 1)
-
-    def relay(self):
-        take(self.block(self.down, None), self.rs.at[0])
-        self.go(self.down, 0, self.to(self.up), 2)
-        take(self.block(self.up, None), self.rs.at[1])
-        self.go(self.up, 1, self.to(self.down), 3)
-
-    def last(self):
-        take(self.block(self.far, 0), self.rs.at[2])
-        take(self.block(self.far, 1), self.rs.at[3])
-
-    def sent(self):
-        take(self.block(self.i, None), self.ss.at[0])
-        take(self.block(self.i, None), self.ss.at[1])
-        take(self.block(self.down, 0), self.ss.at[2])
-        take(self.block(self.up, 1), self.ss.at[3])
-
-
-class Scatter:
-    def __init__(self, block, i, axis_to, ss, rs, part, low, high):
-        self.block, self.i, self.to, self.ss, self.rs = block, i, axis_to, ss, rs
-        self.part, self.low, self.high = part, low, high
-        self.up, self.down, self.far = lax.rem(i + 1, 4), lax.rem(i + 3, 4), lax.rem(i + 2, 4)
-
     def go(self, src, dst, target, k):
-        send(src, dst, self.ss.at[k], self.rs.at[k], target)
+        send(src, dst, self.ss, self.rs.at[k], target)
 
     def first(self):
         up, down = self.to(self.up), self.to(self.down)
         self.go(self.block(self.far, 0), self.part(0), up, 0)
-        self.go(self.block(self.far, 1), self.part(1), down, 1)
-        self.go(self.block(self.up, 1), self.low(1), up, 2)
-        self.go(self.block(self.down, 0), self.high(0), down, 3)
+        self.go(self.block(self.far, 1), self.part(1), down, 0)
+        self.go(self.block(self.up, 1), self.came(0, 1), up, 1)
+        self.go(self.block(self.down, 0), self.came(1, 0), down, 1)
 
     def relay(self):
-        for k, (member, target, half, dst) in enumerate(
-            ((self.up, self.up, 0, self.low(0)), (self.down, self.down, 1, self.high(1)))
+        take(self.parts, self.rs.at[0])
+        for member, half, dst in (
+            (self.up, 0, self.came(0, 0)),
+            (self.down, 1, self.came(1, 1)),
         ):
-            take(self.part(half), self.rs.at[k])
             ref = self.block(member, half)
             ref[...] = (ref[...].astype(F32) + self.part(half)[...].astype(F32)).astype(BF16)
-            self.go(ref, dst, self.to(target), 4 + k)
+            self.go(ref, dst, self.to(member), 1)
 
     def last(self):
-        take(self.low(1), self.rs.at[2])
-        take(self.high(0), self.rs.at[3])
-        take(self.low(0), self.rs.at[4])
-        take(self.high(1), self.rs.at[5])
+        take(self.all_came, self.rs.at[1])
 
     def total(self, half):
         return (
             self.block(self.i, half)[...].astype(F32)
-            + self.low(half)[...].astype(F32)
-            + self.high(half)[...].astype(F32)
-        )
-
-    def sent(self):
-        for k in range(6):
-            take(self.part(0), self.ss.at[k])
+            + self.came(0, half)[...].astype(F32)
+            + self.came(1, half)[...].astype(F32)
+        )
+
+
+class Direct:
+    def __init__(self, block, i, axis_to, ss, rs, slot, slots):
+        self.block, self.i, self.to, self.ss, self.rs = block, i, axis_to, ss, rs
+        self.slot, self.slots = slot, slots
+
+    def first(self):
+        for v in (2, 1, 3):
+            target = lax.rem(self.i + v, SIDE)
+            send(self.block(target), self.slot(v - 1), self.ss, self.rs, self.to(target))
+
+    def total(self):
+        take(self.slots, self.rs)
+        value = self.block(self.i)[...].astype(F32)
+        for v in range(SIDE - 1):
+            value += self.slot(v)[...].astype(F32)
+        return value
 
 
 def softplus(v):
@@ -159,17 +191,15 @@
     act,
     part,
     t_buf,
-    lo_buf,
-    hi_buf,
+    c_buf,
     s_buf,
     t2_buf,
-    lo2_buf,
-    hi2_buf,
     back,
     arrived,
     dn,
     d_mix,
     rows_f,
+    powers,
     lead,
     leads,
     trail,
@@ -221,8 +251,16 @@
     y, x = lax.div(tp, SIDE), lax.rem(tp, SIDE)
     nz = ns // 2
     tokens = norm.shape[0]
-    near = nz // 2
-    chunk = near * 2 * CAP
+    first_chip = [sum(CHUNKS[:k]) for k in range(len(CHUNKS) + 1)]
+    row_count = [n * 2 * CAP for n in CHUNKS]
+    row_base = [n * 2 * CAP for n in first_chip]
+    by_distance = [0] + [d for v in range(1, nz // 2) for d in (v, -v)] + [nz // 2]
+
+    def place(d):
+        return by_distance.index(d)
+
+    def chunk_of(pos):
+        return sum(pos >= first for first in first_chip[1:-1])
 
     def to_x(v):
         return {"sp": sp, "tp": y * SIDE + v}
@@ -234,16 +272,8 @@
         return {"sp": v, "tp": tp}
 
     barrier = pltpu.get_barrier_semaphore()
-    steps = [1, -1, 2, -2, 3, -3]
-    steps = [d for d in steps] + [-4] + [4, 5, -5, 6, -6, 7, -7, 8]
+    steps = by_distance[1:]
     others = [(0, 1)] + [(d, c) for d in steps for c in (0, 1)]
-
-    def far_first(pairs):
-        near_ones = [p for p in pairs if place(p[0]) < near]
-        return near_ones[::-1] + [p for p in pairs if place(p[0]) >= near][::-1]
-
-    def place(d):
-        return (SHIFT - d) % nz
 
     def other(d, c):
         if d == 0:
@@ -327,19 +357,19 @@
     def rows_at(pos, c):
         return pl.ds(pl.multiple_of((pos * 2 + c) * CAP, CAP), CAP)
 
-    for d, c in far_first(others):
+    by_chunk = [[p for p in others if chunk_of(place(p[0])) == k] for k in range(len(CHUNKS))]
+    for k, (d, c) in [(k, p) for k, pairs in enumerate(by_chunk) for p in pairs[::-1]]:
         target = other(d, c)
-        k = 0 if place(d) < near else 1
         send(
             packed.at[:, pl.ds(pl.multiple_of(target * CAP, CAP), CAP), :],
             rows.at[:, y, rows_at(place(d), core), own_x],
-            z_s.at[k],
+            z_s,
             z_r.at[k],
             to_sp(target),
         )
     pltpu.make_async_copy(
         packed.at[:, pl.ds(pl.multiple_of(sp * CAP, CAP), CAP), :],
-        rows.at[:, y, rows_at(SHIFT, core), own_x],
+        rows.at[:, y, rows_at(0, core), own_x],
         z_r.at[0],
     ).start()
 
@@ -357,6 +387,8 @@
     def moved(v, step, fill):
         inside = token >= step if step > 0 else token < tokens + step
         return jnp.where(inside, pltpu.roll(v, step % tokens, 1), fill)
+
+    levels = tokens.bit_length() - 1
 
     def scan(a, b, sign):
         step = 1
@@ -385,41 +417,47 @@
         rows_f[0] = keep_cum
         rows_f[1] = state_loc
         rows_f[2] = keep
-        rows_f[3] = moved(keep, -1, 1.0)
+        tail = moved(keep, -1, 1.0)
+        for level in range(levels):
+            powers[level] = tail
+            tail = tail * moved(tail, -(1 << level), 1.0)
+        rows_f[3] = tail
         rows_f[4] = scale_in * admit
         rows_f[5] = scale_in * signal * admit * (1.0 - admit)
         rows_f[6] = admit * signal * keep * keep / scale_in
         rows_f[7] = speed * retain * (1.0 - retain)
 
     def z_arrived(k):
-        with jax.named_scope(f"z_arrived{k}"):
-            take(rows.at[:, y, pl.ds(k * chunk, chunk), own_x], z_r.at[k])
-
-    def gathers(k):
-        base, half_rows = k * chunk, chunk // 2
+        take(rows.at[:, y, pl.ds(row_base[k], row_count[k]), own_x], z_r.at[k])
+
+    def at_x(i):
+        return pl.ds(pl.multiple_of(i * COLS, COLS), COLS)
+
+    def flows(k):
+        half_rows = row_count[k] // 2
 
         def span(half):
             if half is None:
-                return pl.ds(base, chunk)
-            return pl.ds(base + half * half_rows, half_rows)
-
-        def at_x(i):
-            return pl.ds(pl.multiple_of(i * COLS, COLS), COLS)
-
-        blocks = (
-            (lambda i, h: rows.at[0, y, span(h), at_x(i)], x, to_x),
-            (lambda i, h: rows.at[1, i, span(h), own_x], y, to_y),
-            (lambda i, h: rows.at[0, i, span(h), :], y, to_y),
-            (lambda i, h: rows.at[1, :, span(h), at_x(i)], x, to_x),
-        )
-        made = [
-            Gather(b, i, to, ag_s.at[4 * k + n], ag_r.at[4 * k + n])
-            for n, (b, i, to) in enumerate(blocks)
-        ]
-        return made[:2], made[2:]
+                return pl.ds(row_base[k], row_count[k])
+            return pl.ds(row_base[k] + half * half_rows, half_rows)
+
+        def bulk(count):
+            return rows.at[0, pl.ds(0, count), span(None), pl.ds(0, COLS)]
+
+        return (
+            Flow(
+                lambda p, q, h: rows.at[0, q, span(h), at_x(p)],
+                bulk, x, y, to_x, to_y, ag_s, ag_r.at[2 * k],
+            ),
+            Flow(
+                lambda p, q, h: rows.at[1, p, span(h), at_x(q)],
+                bulk, y, x, to_y, to_x, ag_s, ag_r.at[2 * k + 1],
+            ),
+        )
 
     def expert(k):
-        span = pl.ds(k * chunk, chunk)
+        chunk = row_count[k]
+        span = pl.ds(row_base[k], chunk)
         deep = rows.shape[3]
         hidden = jnp.zeros((chunk, 2 * COLS), F32)
         d_act = jnp.zeros((chunk, COLS), F32)
@@ -442,110 +480,83 @@
                 part[j, i + 1, span, :] = piece[:, COLS:]
 
     def scatters(k):
-        base, half, quarter = k * chunk, chunk // 2, chunk // 4
+        base, half, quarter = row_base[k], row_count[k] // 2, row_count[k] // 4
 
         def span(start, h):
             return pl.ds(start + h * quarter, quarter)
 
-        def full(buf, n):
-            return lambda h: buf.at[n, :, pl.ds(h * quarter, quarter), :]
-
-        def flat(buf, n):
-            return lambda h: buf.at[n, pl.ds(h * quarter, quarter), :]
-
-        n = 2 * k
-        made = (
-            Scatter(
-                lambda i, h: part.at[:, i, span(base, h), :], x, to_x,
-                rs_s.at[4 * k], rs_r.at[4 * k],
-                lambda h: t_buf.at[n, h], full(lo_buf, n), full(hi_buf, n),
-            ),
-            Scatter(
-                lambda i, h: part.at[i, :, span(base + half, h), :], y, to_y,
-                rs_s.at[4 * k + 1], rs_r.at[4 * k + 1],
-                lambda h: t_buf.at[n + 1, h], full(lo_buf, n + 1), full(hi_buf, n + 1),
-            ),
-            Scatter(
-                lambda i, h: s_buf.at[n, i, pl.ds(h * quarter, quarter), :], y, to_y,
-                rs_s.at[4 * k + 2], rs_r.at[4 * k + 2],
-                lambda h: t2_buf.at[n, h], flat(lo2_buf, n), flat(hi2_buf, n),
-            ),
-            Scatter(
-                lambda i, h: s_buf.at[n + 1, i, pl.ds(h * quarter, quarter), :], x, to_x,
-                rs_s.at[4 * k + 3], rs_r.at[4 * k + 3],
-                lambda h: t2_buf.at[n + 1, h], flat(lo2_buf, n + 1), flat(hi2_buf, n + 1),
-            ),
-        )
-        return made[:2], made[2:]
+        def make(n, block, i, axis_to, i2, axis_to2):
+            one = Scatter(
+                block, i, axis_to, rs_s.at[0], rs_r.at[n],
+                lambda h: t_buf.at[n, h, :, pl.ds(0, quarter), :],
+                lambda v, h: c_buf.at[n, v, :, pl.ds(h * quarter, quarter), :],
+                t_buf.at[n, :, :, pl.ds(0, quarter), :],
+                c_buf.at[n, :, :, pl.ds(0, half), :],
+            )
+            two = Direct(
+                lambda m: s_buf.at[n, m, pl.ds(0, half), :], i2, axis_to2,
+                rs_s.at[1], rs_r.at[n, 2],
+                lambda v: t2_buf.at[n, v, pl.ds(0, half), :],
+                t2_buf.at[n, :, pl.ds(0, half), :],
+            )
+            return one, two
+
+        a1, a2 = make(
+            2 * k, lambda i, h: part.at[:, i, span(base, h), :], x, to_x, y, to_y
+        )
+        b1, b2 = make(
+            2 * k + 1, lambda i, h: part.at[i, :, span(base + half, h), :], y, to_y, x, to_x
+        )
+        return (a1, b1), (a2, b2)
 
     def between(k, first):
-        quarter = chunk // 4
+        quarter = row_count[k] // 4
         for n, ring in enumerate(first):
             for h in (0, 1):
                 s_buf[2 * k + n, :, pl.ds(h * quarter, quarter), :] = ring.total(h).astype(BF16)
 
     def give_back(k, second):
-        half, quarter = chunk // 2, chunk // 4
+        half = row_count[k] // 2
         for n, ring in enumerate(second):
-            for h in (0, 1):
-                back[pl.ds(k * chunk + n * half + h * quarter, quarter), :] = ring.total(h).astype(
-                    BF16
-                )
+            back[pl.ds(row_base[k] + n * half, half), :] = ring.total().astype(BF16)
         dst = arrived.at[pl.ds(pl.multiple_of(sp * CAP, CAP), CAP), :]
         for d, c in others[::-1]:
-            pos = place(-d)
-            if (pos < near) != (k == 0):
+            pos = place(-d if 0 < abs(d) < nz // 2 else d)
+            if chunk_of(pos) != k:
                 continue
             where = rows_at(pos, 1 - core if d == 0 else c)
-            send(back.at[where, :], dst, back_s.at[k], back_r, to_sp(other(d, c)))
+            send(back.at[where, :], dst, back_s, back_r, to_sp(other(d, c)))
         if k == 0:
-            pltpu.make_async_copy(back.at[rows_at(SHIFT, core), :], dst, back_r).start()
-
-    def each(rings, name, label=""):
-        with jax.named_scope(label + name):
-            for ring in rings:
-                getattr(ring, name)()
-
-    a0, b0 = gathers(0)
-    a1, b1 = gathers(1)
-    r0, q0 = scatters(0)
-    r1, q1 = scatters(1)
-
-    z_arrived(0)
-    each(a0, "first", "a0_")
-    each(a0, "relay", "a0_")
-    each(a0, "last", "a0_")
-    each(b0, "first", "b0_")
-    z_arrived(1)
-    each(a1, "first", "a1_")
-    each(b0, "relay", "b0_")
-    each(a1, "relay", "a1_")
-    each(b0, "last", "b0_")
-    each(a1, "last", "a1_")
-    each(b1, "first", "b1_")
-    have(9, 15)
-    with jax.named_scope("expert0"):
-        expert(0)
-    each(r0, "first", "r0_")
-    each(b1, "relay", "b1_")
-    each(r0, "relay", "r0_")
-    each(r0, "last", "r0_")
-    between(0, r0)
-    each(q0, "first", "q0_")
-    each(b1, "last", "b1_")
-    with jax.named_scope("expert1"):
-        expert(1)
-    each(r1, "first", "r1_")
-    each(q0, "relay", "q0_")
-    each(q0, "last", "q0_")
-    give_back(0, q0)
-    each(r1, "relay", "r1_")
-    each(r1, "last", "r1_")
-    between(1, r1)
-    each(q1, "first", "q1_")
-    each(q1, "relay", "q1_")
-    each(q1, "last", "q1_")
-    give_back(1, q1)
+            pltpu.make_async_copy(back.at[rows_at(0, core), :], dst, back_r).start()
+
+    all_flows = [flows(k) for k in range(len(CHUNKS))]
+    all_sums = [scatters(k) for k in range(len(CHUNKS))]
+
+    def both_of(pair, name, *given):
+        for one_of in pair:
+            getattr(one_of, name)(*given)
+
+    for number, (step, k, *given) in enumerate(ORDER):
+        with jax.named_scope(f"{step}{k}" + "".join(f"_{m}" for m in given)):
+            if step == "begin":
+                z_arrived(k)
+                both_of(all_flows[k], "start")
+            elif step == "expert":
+                if number == FIRST_EXPERT:
+                    have(9, 15)
+                both_of(all_flows[k], "last")
+                expert(k)
+                both_of(all_sums[k][0], "first")
+            elif step == "mid":
+                both_of(all_sums[k][0], "relay")
+            elif step == "turn":
+                both_of(all_sums[k][0], "last")
+                between(k, all_sums[k][0])
+                both_of(all_sums[k][1], "first")
+            elif step == "give":
+                give_back(k, all_sums[k][1])
+            else:
+                both_of(all_flows[k], step, *given)
 
     with jax.named_scope("grads"):
         deep = rows.shape[3]
@@ -561,6 +572,15 @@
         )
         for copy in stored:
             copy.start()
+
+    with jax.named_scope("sent"):
+        all_rows = ns * CAP
+        take(packed.at[:, pl.ds(0, all_rows - CAP), :], z_s)
+        take(rows.at[:, :, pl.ds(0, all_rows // 16 * 15), :], ag_s)
+        take(part.at[pl.ds(0, 3)], rs_s.at[0])
+        take(part.at[0, pl.ds(0, 3)], rs_s.at[1])
+        take(back.at[pl.ds(0, all_rows - CAP), :], back_s)
+        take(leads.at[pl.ds(0, ns - 1)], lead_s)
 
     with jax.named_scope("lead_wait"):
         take(leads.at[pl.ds(0, ns - 1)], lead_r)
@@ -589,7 +609,7 @@
         ref = spot(n, i, j)
         for v in (2, 1, 3):
             target = to_x(lax.rem(x + v, SIDE)) if along_x else to_y(lax.rem(y + v, SIDE))
-            send(ref, ref, dn_s.at[n, slot, v - 1], dn_r.at[n, slot, v - 1], target)
+            send(ref, ref, dn_s, dn_r.at[n, v - 1 if slot == 0 else 3], target)
 
     def back_by(p, v):
         return lax.rem(p + SIDE - v, SIDE)
@@ -602,16 +622,11 @@
         for v in (1, 3, 2):
             for n in (0, 1):
                 i, j = (back_by(x, v), y) if n == 0 else (x, back_by(y, v))
-                take(spot(n, i, j), dn_r.at[n, 0, v - 1])
+                take(spot(n, i, j), dn_r.at[n, v - 1])
                 spread(n, i, j, n == 1, 1 + v)
     with jax.named_scope("dn_last"):
-        for v in (0, 1, 3, 2):
-            for w in (1, 3, 2):
-                for n in (0, 1):
-                    i, j = (
-                        (back_by(x, v), back_by(y, w)) if n == 0 else (back_by(x, w), back_by(y, v))
-                    )
-                    take(spot(n, i, j), dn_r.at[n, 1 + v, w - 1])
+        for n in (0, 1):
+            take(dn.at[pl.ds(0, 3), pl.ds(0, half), :], dn_r.at[n, 3])
 
     with jax.named_scope("mix"):
         inv_rms = upright(irms[...])
@@ -631,15 +646,6 @@
             )
             d_mix[:, cols] = mix.astype(BF16)
 
-    with jax.named_scope("trail"):
-        d_state = dot(out_m[...], d_mix[...], 1, 1)
-        tail, grad_loc = scan(rows_f[3], d_state, -1)
-        first_grad = lying(rows_f[2][:, :1] * grad_loc[:, :1])
-        trail[...] = jnp.concatenate([first_grad, first_grad], axis=1)
-        trails[sp] = trail[...]
-        for d, c in others:
-            send(trail, trails.at[sp], trail_s, trail_r, to_sp(other(d, c)))
-
     with jax.named_scope("gw_dot"):
         wide_piece = 2 * g_out.shape[0]
         gw = dot(hidden, d_mix[...], 1, 0)
@@ -651,6 +657,17 @@
             gw_all[1, n] = jnp.concatenate([top[:, cut:], low[:, cut:]], axis=1).astype(BF16)
 
     send(gw_all.at[1 - core], gw_pair, pair_s, pair_r, to_sp(z * 2 + 1 - core))
+    with jax.named_scope("trail"):
+        d_state = dot(out_m[...], d_mix[...], 1, 1)
+        grad_loc = d_state
+        for level in range(levels):
+            grad_loc += powers[level] * moved(grad_loc, -(1 << level), 0.0)
+        first_grad = lying(rows_f[2][:, :1] * grad_loc[:, :1])
+        trail[...] = jnp.concatenate([first_grad, first_grad], axis=1)
+        trails[sp] = trail[...]
+        for d, c in others:
+            send(trail, trails.at[sp], trail_s, trail_r, to_sp(other(d, c)))
+
     with jax.named_scope("pair_wait"):
         take(gw_pair, pair_r)
     gw_chip[...] = (gw_all[core].astype(F32) + gw_pair[...].astype(F32)).astype(BF16)
@@ -658,12 +675,15 @@
         zz = lax.rem(z + d + nz, nz)
         send(gw_chip.at[zz], gw_in.at[z], gw_s, gw_r, to_sp(zz * 2 + core))
     pltpu.make_async_copy(gw_chip.at[z], gw_in.at[z], gw_r).start()
+    take(rows.at[0, 0, pl.ds(0, rows.shape[2] // 16 * 15), :], dn_s)
+    for copy in stored:
+        copy.wait()
     with jax.named_scope("trail_wait"):
         take(trails.at[pl.ds(0, ns - 1)], trail_r)
     entering = jnp.zeros((1, channels), F32)
     for i in range(ns):
         entering += coef[i] * trails[i][:, :channels]
-    total = grad_loc + tail * standing(entering)
+    total = grad_loc + rows_f[3] * standing(entering)
     g_rec[...] = total * rows_f[4]
     g_in[...] = total * rows_f[5]
     g_dec[...] = total * rows_f[6]
@@ -675,20 +695,6 @@
     cut = g_out.shape[0]
     g_out[...] = jnp.concatenate([acc[:, :cut], acc[:, cut:]], axis=0).T
 
-    for copy in stored:
-        copy.wait()
-    block = ns // 2 * CAP
-    take(packed.at[:, pl.ds(0, block - CAP), :], z_s.at[0])
-    take(packed.at[:, pl.ds(0, block), :], z_s.at[1])
-    for ring in a0 + b0 + a1 + b1 + list(r0) + list(q0) + list(r1) + list(q1):
-        ring.sent()
-    for n in (0, 1):
-        for slot in range(5):
-            for v in range(3):
-                take(spot(n, x, y), dn_s.at[n, slot, v])
-    take(back.at[pl.ds(0, block - CAP), :], back_s.at[0])
-    take(back.at[pl.ds(0, block), :], back_s.at[1])
-    take(leads.at[pl.ds(0, ns - 1)], lead_s)
     take(trails.at[pl.ds(0, ns - 1)], trail_s)
     take(gw_pair, pair_s)
     take(gw_in.at[pl.ds(0, nz - 1)], gw_s)
@@ -728,7 +734,8 @@
     tokens, features = normed.shape
     channels = recurrence_input.shape[1]
     slots = ns * CAP
-    chunk, quarter = slots // 2, slots // 8
+    chunks = len(CHUNKS)
+    quarter = max(CHUNKS) * 2 * CAP // 4
     wide = features // SIDE
     vmem, dma = pltpu.VMEM, pltpu.SemaphoreType.DMA
     args = (
@@ -771,18 +778,16 @@
             vmem((slots, 2 * COLS), BF16),
             vmem((slots, COLS), BF16),
             vmem((SIDE, SIDE, slots, COLS), BF16),
-            vmem((4, 2, SIDE, quarter, COLS), BF16),
-            vmem((4, SIDE, 2 * quarter, COLS), BF16),
-            vmem((4, SIDE, 2 * quarter, COLS), BF16),
-            vmem((4, SIDE, 2 * quarter, COLS), BF16),
-            vmem((4, 2, quarter, COLS), BF16),
-            vmem((4, 2 * quarter, COLS), BF16),
-            vmem((4, 2 * quarter, COLS), BF16),
+            vmem((2 * chunks, 2, SIDE, quarter, COLS), BF16),
+            vmem((2 * chunks, 2, SIDE, 2 * quarter, COLS), BF16),
+            vmem((2 * chunks, SIDE, 2 * quarter, COLS), BF16),
+            vmem((2 * chunks, 3, 2 * quarter, COLS), BF16),
             vmem((slots, COLS), BF16),
             vmem((slots, COLS), BF16),
             vmem((SIDE, tokens, wide), BF16),
             vmem((tokens, features), BF16),
             vmem((8, channels, tokens), F32),
+            vmem((tokens.bit_length() - 1, channels, tokens), F32),
             vmem((1, 2 * channels), F32),
             vmem((ns, 1, 2 * channels), F32),
             vmem((1, 2 * channels), F32),
@@ -800,15 +805,15 @@
             *(vmem(a.shape, a.dtype) for a in args[9:]),
             dma((len(args),)),
             dma((3,)),
+            dma,
+            dma((chunks,)),
+            dma,
+            dma((2 * chunks, 7)),
             dma((2,)),
-            dma((2,)),
-            dma((8, 4)),
-            dma((8, 4)),
-            dma((8, 6)),
-            dma((8, 6)),
-            dma((2, 5, 3)),
-            dma((2, 5, 3)),
-            dma((2,)),
+            dma((2 * chunks, 3)),
+            dma,
+            dma((2, 4)),
+            dma,
             dma,
             dma,
             dma,

time: 115 us -> 99.3 us (0.86)
  Pallas kernels: 114 us -> 98.4 us
    pallas_call x1, Pallas kernels: 112 us -> 96.1 us  [shards(): pl.pallas_call(functools.partial(kernel, ns), out_shape=(jax.ShapeDtypeSt...]
where the time goes in v3:
time: 99.3 us; the launch traced here: 99.1 us
  Pallas kernels  98.4 us (99%)
    pallas_call x1, Pallas kernels, shards(): pl.pallas_call(functools.partial(kernel, ns), out_shape=(jax.ShapeDtypeSt...  96.1 us
    pallas_call x1, Pallas kernels, shards(): pl.pallas_call(functools.partial(finish, len(results)), out_shape=tuple((...  2.33 us

profile of v3, /device:TPU:1, one launch (start us, length us, event | category | flops | bytes accessed | tf_op | source)
XLA Modules:
  0.0 99.1 jit_solution(14871746820686650234)
XLA Ops:
  0.6 96.1 %shard_map.198 = (bf16[1,2048,128]{2,1,0:T(8,128)(2,1)}, bf16[1,2048,128]{2,1,0:T(8,128)(2,1)}, bf16[1,128,2048]{2,1,0:T(8,128)(2,1)}, f32[64,64]{1,0:T(8,128)},...) custom-call(bf16[128,2048]{1,0:T(8,128)(2,1)} %cot_h.1, bf16[128,2048]{1,0:T(8,128)(2,1)} %norm_h.1, ...), custom_call_target="tpu_custom_call" | custom-call | tf_op jit(solution)/shard_map/pallas_call | solution.py:760
  96.8 2.3 %shard_map.199 = (bf16[1,2048,128]{2,1,0:T(8,128)(2,1)}, bf16[1,2048,128]{2,1,0:T(8,128)(2,1)}, bf16[1,128,2048]{2,1,0:T(8,128)(2,1)}, f32[64,64]{1,0:T(8,128)},...) custom-call(bf16[1,2048,128]{2,1,0:T(8,128)(2,1)} %get-tuple-element.21.refs_0_, ...), custom_call_target="tpu_custom_call" | custom-call | tf_op jit(solution)/shard_map/pallas_call | solution.py:831

commit v4 on v3

--- a/solution.py
+++ b/solution.py
@@ -12,6 +12,7 @@
 BF16 = jnp.bfloat16
 SIDE = 4
 CHUNKS = (4, 6, 4, 2)
+SOURCES = (1, -1, 2, -2, 4, -4, 5, -5, 6, -6, 7, -7, 8, 3, 0, -3)
 COLS = 128
 ORDER = (('begin', 0), ('near', 0), ('relay', 0, 0), ('begin', 1), ('across', 0), ('relay', 0, 2), ('relay', 0, 1), ('near', 1), ('relay', 1, 0), ('relay', 0, 3), ('begin', 2), ('across', 1), ('relay', 1, 2), ('relay', 1, 1), ('begin', 3), ('expert', 0), ('near', 2), ('relay', 2, 0), ('relay', 1, 3), ('near', 3), ('relay', 3, 0), ('mid', 0), ('across', 2), ('relay', 2, 2), ('relay', 2, 1), ('expert', 1), ('across', 3), ('relay', 3, 2), ('relay', 3, 1), ('turn', 0), ('relay', 2, 3), ('mid', 1), ('relay', 3, 3), ('expert', 2), ('give', 0), ('turn', 1), ('expert', 3), ('mid', 2), ('give', 1), ('mid', 3), ('turn', 2), ('turn', 3), ('give', 2), ('give', 3))
 FIRST_EXPERT = [step for step, *_ in ORDER].index("expert")
@@ -254,10 +255,10 @@
     first_chip = [sum(CHUNKS[:k]) for k in range(len(CHUNKS) + 1)]
     row_count = [n * 2 * CAP for n in CHUNKS]
     row_base = [n * 2 * CAP for n in first_chip]
-    by_distance = [0] + [d for v in range(1, nz // 2) for d in (v, -v)] + [nz // 2]
+    home = SOURCES.index(0)
 
     def place(d):
-        return by_distance.index(d)
+        return SOURCES.index(d)
 
     def chunk_of(pos):
         return sum(pos >= first for first in first_chip[1:-1])
@@ -272,8 +273,8 @@
         return {"sp": v, "tp": tp}
 
     barrier = pltpu.get_barrier_semaphore()
-    steps = by_distance[1:]
-    others = [(0, 1)] + [(d, c) for d in steps for c in (0, 1)]
+    steps = [d for d in SOURCES if d != 0]
+    others = [(d, c) for d in SOURCES for c in (0, 1) if (d, c) != (0, 0)]
 
     def other(d, c):
         if d == 0:
@@ -369,8 +370,8 @@
         )
     pltpu.make_async_copy(
         packed.at[:, pl.ds(pl.multiple_of(sp * CAP, CAP), CAP), :],
-        rows.at[:, y, rows_at(0, core), own_x],
-        z_r.at[0],
+        rows.at[:, y, rows_at(home, core), own_x],
+        z_r.at[chunk_of(home)],
     ).start()
 
     channels = extra.shape[0]
@@ -526,8 +527,8 @@
                 continue
             where = rows_at(pos, 1 - core if d == 0 else c)
             send(back.at[where, :], dst, back_s, back_r, to_sp(other(d, c)))
-        if k == 0:
-            pltpu.make_async_copy(back.at[rows_at(0, core), :], dst, back_r).start()
+        if k == chunk_of(home):
+            pltpu.make_async_copy(back.at[rows_at(home, core), :], dst, back_r).start()
 
     all_flows = [flows(k) for k in range(len(CHUNKS))]
     all_sums = [scatters(k) for k in range(len(CHUNKS))]
@@ -671,7 +672,7 @@
     with jax.named_scope("pair_wait"):
         take(gw_pair, pair_r)
     gw_chip[...] = (gw_all[core].astype(F32) + gw_pair[...].astype(F32)).astype(BF16)
-    for d in steps[::-1]:
+    for d in sorted(steps, key=abs)[::-1]:
         zz = lax.rem(z + d + nz, nz)
         send(gw_chip.at[zz], gw_in.at[z], gw_s, gw_r, to_sp(zz * 2 + core))
     pltpu.make_async_copy(gw_chip.at[z], gw_in.at[z], gw_r).start()

time: 99.3 us -> 98 us (0.987); the launches traced: 99.1 us -> 96.7 us
  Pallas kernels: 98.4 us -> 96.1 us
    pallas_call x1, Pallas kernels: 96.1 us -> 93.7 us  [shards(): pl.pallas_call(functools.partial(kernel, ns), out_shape=(jax.ShapeDtypeSt...]
where the time goes in v4:
time: 98 us; the launch traced here: 96.7 us
  Pallas kernels  96.1 us (98%)
    pallas_call x1, Pallas kernels, shards(): pl.pallas_call(functools.partial(kernel, ns), out_shape=(jax.ShapeDtypeSt...  93.7 us
    pallas_call x1, Pallas kernels, shards(): pl.pallas_call(functools.partial(finish, len(results)), out_shape=tuple((...  2.33 us

profile of v4, /device:TPU:1, one launch (start us, length us, event | category | flops | bytes accessed | tf_op | source)
XLA Modules:
  0.0 96.7 jit_solution(8273005130291593856)
XLA Ops:
  0.6 93.7 %shard_map.198 = (bf16[1,2048,128]{2,1,0:T(8,128)(2,1)}, bf16[1,2048,128]{2,1,0:T(8,128)(2,1)}, bf16[1,128,2048]{2,1,0:T(8,128)(2,1)}, f32[64,64]{1,0:T(8,128)},...) custom-call(bf16[128,2048]{1,0:T(8,128)(2,1)} %cot_h.1, bf16[128,2048]{1,0:T(8,128)(2,1)} %norm_h.1, ...), custom_call_target="tpu_custom_call" | custom-call | tf_op jit(solution)/shard_map/pallas_call | solution.py:761
  94.4 2.3 %shard_map.199 = (bf16[1,2048,128]{2,1,0:T(8,128)(2,1)}, bf16[1,2048,128]{2,1,0:T(8,128)(2,1)}, bf16[1,128,2048]{2,1,0:T(8,128)(2,1)}, f32[64,64]{1,0:T(8,128)},...) custom-call(bf16[1,2048,128]{2,1,0:T(8,128)(2,1)} %get-tuple-element.21.refs_0_, ...), custom_call_target="tpu_custom_call" | custom-call | tf_op jit(solution)/shard_map/pallas_call | solution.py:832

commit v5 on v4

--- a/solution.py
+++ b/solution.py
@@ -666,7 +666,7 @@
         first_grad = lying(rows_f[2][:, :1] * grad_loc[:, :1])
         trail[...] = jnp.concatenate([first_grad, first_grad], axis=1)
         trails[sp] = trail[...]
-        for d, c in others:
+        for d, c in sorted(others, key=lambda pair: -abs(pair[0])):
             send(trail, trails.at[sp], trail_s, trail_r, to_sp(other(d, c)))
 
     with jax.named_scope("pair_wait"):

time: 98 us -> 98 us (level)
  no operation moved by 1% of the time
where the time goes in v5:
time: 98 us; the launch traced here: 96.4 us
  Pallas kernels  95.7 us (98%)
    pallas_call x1, Pallas kernels, shards(): pl.pallas_call(functools.partial(kernel, ns), out_shape=(jax.ShapeDtypeSt...  93.4 us
    pallas_call x1, Pallas kernels, shards(): pl.pallas_call(functools.partial(finish, len(results)), out_shape=tuple((...  2.33 us

profile of v5, /device:TPU:1, one launch (start us, length us, event | category | flops | bytes accessed | tf_op | source)
XLA Modules:
  0.0 96.4 jit_solution(5735425971058521020)
XLA Ops:
  0.6 93.4 %shard_map.198 = (bf16[1,2048,128]{2,1,0:T(8,128)(2,1)}, bf16[1,2048,128]{2,1,0:T(8,128)(2,1)}, bf16[1,128,2048]{2,1,0:T(8,128)(2,1)}, f32[64,64]{1,0:T(8,128)},...) custom-call(bf16[128,2048]{1,0:T(8,128)(2,1)} %cot_h.1, bf16[128,2048]{1,0:T(8,128)(2,1)} %norm_h.1, ...), custom_call_target="tpu_custom_call" | custom-call | tf_op jit(solution)/shard_map/pallas_call | solution.py:761
  94.0 2.3 %shard_map.199 = (bf16[1,2048,128]{2,1,0:T(8,128)(2,1)}, bf16[1,2048,128]{2,1,0:T(8,128)(2,1)}, bf16[1,128,2048]{2,1,0:T(8,128)(2,1)}, f32[64,64]{1,0:T(8,128)},...) custom-call(bf16[1,2048,128]{2,1,0:T(8,128)(2,1)} %get-tuple-element.21.refs_0_, ...), custom_call_target="tpu_custom_call" | custom-call | tf_op jit(solution)/shard_map/pallas_call | solution.py:832
